TPU v7x, 32 devices: a whole 2x2x4 slice. The times are simulated.
32 devices in a mesh: sp: 8 (over z, x), tp: 4 (over y, core).
Axes of the slice: x: 2, y: 2, z: 4, core: 2. Of those that a mesh axis runs over, the one named last changes fastest.
Arguments:
- broad_probe_tensor: bfloat16 [4096, 1024], P('sp', 'tp'), may hold values from -6 to 6
- broad_lookup_tensor: bfloat16 [4096, 1024], P('sp', 'tp'), may hold values from -6 to 6
- broad_payload_tensor: bfloat16 [4096, 1024], P('sp', 'tp'), may hold values from -6 to 6
- broad_emission_valve: bfloat16 [4096, 1024], P('sp', 'tp'), may hold values from -6 to 6
- slim_probe_tensor: bfloat16 [4096, 1024], P('sp', 'tp'), may hold values from -6 to 6
- slim_lookup_tensor: bfloat16 [4096, 1024], P('sp', 'tp'), may hold values from -6 to 6
- slim_payload_tensor: bfloat16 [4096, 1024], P('sp', 'tp'), may hold values from -6 to 6
- slim_emission_valve: bfloat16 [4096, 1024], P('sp', 'tp'), may hold values from -6 to 6
- broad_forgetting_speed: float32 [8], P('tp'), may hold values from -0.08 to 0
- slim_forgetting_speed: float32 [16], P('tp'), may hold values from -0.08 to 0
- broad_channel_scaling: float32 [1024], P('tp'), may hold values from 0.1 to 1.9
- slim_channel_scaling: float32 [1024], P('tp'), may hold values from 0.1 to 1.9
- surge_forgetting: float32 [4096], P('sp'), may hold values from -2.1 to 0
- broad_emission_proj: bfloat16 [1024, 2048], replicated, may hold values from -0.125 to 0.125
- slim_emission_proj: bfloat16 [1024, 2048], replicated, may hold values from -0.125 to 0.125
- skip_stream: bfloat16 [4096, 2048], P(('sp', 'tp')), may hold values from -6 to 6
- premix_scaling_coeffs: float32 [2048], replicated, may hold values from 0.1 to 1.9
- routed_specialist_ids: int32 [4096, 2], P('sp'), may hold values from 0 to 7, as said below
- routed_specialist_shares: float32 [4096, 2], P('sp'), may hold values from 0.2 to 1
- specialist_valve_proj: bfloat16 [8, 2048, 2048], P('sp', None, 'tp'), may hold values from -0.125 to 0.125
- specialist_expand_proj: bfloat16 [8, 2048, 2048], P('sp', None, 'tp'), may hold values from -0.125 to 0.125
- specialist_contract_proj: bfloat16 [8, 2048, 2048], P('sp', 'tp'), may hold values from -0.125 to 0.125
Outputs:
- result: bfloat16 [4096, 2048], P(('sp', 'tp'))
Inputs may be any that keep to these rules, and one draw needn't show every extreme that they name: `routed_specialist_ids`: each row names two different experts of one group, that is of the same run of 2 consecutive experts. The rows of one device (each aligned block of 128 rows) name each expert at most 64 times, and some expert is named exactly 64 times by the rows of every device.
All inputs are finite; a program needn't handle non-finite values.
Results may differ from a plain program's by a relative error of at most 0.018.
Values may be sent and summed in bfloat16 or wider, within the bound.
A program may use at most 128 MiB of HBM per device.

v0:
```python
import jax
import jax.numpy as jnp
from jax import lax
from jax.experimental import pallas as pl
from jax.experimental.pallas import tpu as pltpu
from jax.sharding import PartitionSpec as P

MESH = pl.DeviceIdType.MESH
VMEM_SPEC = pl.BlockSpec(memory_space=pltpu.VMEM)

BROAD_CHANNEL_DIM = 128
THIN_CHANNEL_DIM = 64
GROUPS = 4


rope_base = 10000.0
epsilon = 1e-06


def exchange_kernel(state_ref, tile_ref, states_ref, tiles_ref, send_sem, recv_sem):
    me = lax.axis_index("sp")
    count = states_ref.shape[0]
    barrier = pltpu.get_barrier_semaphore()
    for step in range(1, count):
        pl.semaphore_signal(
            barrier, inc=1, device_id={"sp": lax.rem(me + step, count)}, device_id_type=MESH
        )
    pl.semaphore_wait(barrier, count - 1)
    copies = []
    for step in range(1, count):
        for kind, (src, dst) in enumerate(((state_ref, states_ref), (tile_ref, tiles_ref))):
            copy = pltpu.make_async_remote_copy(
                src_ref=src,
                dst_ref=dst.at[me],
                send_sem=send_sem.at[kind, step],
                recv_sem=recv_sem.at[kind, step],
                device_id={"sp": lax.rem(me + step, count)},
                device_id_type=MESH,
            )
            copy.start()
            copies.append(copy)
    states_ref[me] = state_ref[...]
    tiles_ref[me] = tile_ref[...]
    for copy in copies:
        copy.wait()


def exchange(state, tile):
    count = lax.axis_size("sp")
    return pl.pallas_call(
        exchange_kernel,
        out_shape=(
            jax.ShapeDtypeStruct((count,) + state.shape, state.dtype),
            jax.ShapeDtypeStruct((count,) + tile.shape, tile.dtype),
        ),
        in_specs=[VMEM_SPEC] * 2,
        out_specs=(VMEM_SPEC, VMEM_SPEC),
        scratch_shapes=[
            pltpu.SemaphoreType.DMA((2, count)),
            pltpu.SemaphoreType.DMA((2, count)),
        ],
        compiler_params=pltpu.CompilerParams(collective_id=0, has_side_effects=True),
        name="state_exchange",
    )(state, tile)


def greet_group(groups, pair):
    me = lax.axis_index("sp")
    group = me // pair
    member = lax.rem(me, pair)
    barrier = pltpu.get_barrier_semaphore()
    for step in range(1, groups):
        pl.semaphore_signal(
            barrier,
            inc=1,
            device_id={"sp": lax.rem(group + step, groups) * pair + member},
            device_id_type=MESH,
        )
    pl.semaphore_signal(
        barrier, inc=1, device_id={"sp": group * pair + 1 - member}, device_id_type=MESH
    )
    pl.semaphore_wait(barrier, groups)
    return group, member


def dispatch_kernel(rows_ref, out_ref, send_far, recv_far, send_near, recv_near):
    groups = rows_ref.shape[0]
    pair = out_ref.shape[0]
    group, member = greet_group(groups, pair)
    partner = group * pair + 1 - member
    far = []
    for step in range(1, groups):
        target = lax.rem(group + step, groups)
        copy = pltpu.make_async_remote_copy(
            src_ref=rows_ref.at[target],
            dst_ref=out_ref.at[member, group],
            send_sem=send_far.at[step],
            recv_sem=recv_far.at[step],
            device_id={"sp": target * pair + member},
            device_id_type=MESH,
        )
        copy.start()
        far.append(copy)
    near = []
    for step in range(groups):
        origin = lax.rem(group - step + groups, groups)
        if step > 0:
            far[step - 1].wait_recv()
        copy = pltpu.make_async_remote_copy(
            src_ref=rows_ref.at[group] if step == 0 else out_ref.at[member, origin],
            dst_ref=out_ref.at[member, origin],
            send_sem=send_near.at[step],
            recv_sem=recv_near.at[step],
            device_id={"sp": partner},
            device_id_type=MESH,
        )
        copy.start()
        near.append(copy)
        if step == 0:
            out_ref[member, group] = rows_ref[group]
    for copy in far:
        copy.wait_send()
    for copy in near:
        copy.wait()


def dispatch(rows, pair):
    groups = rows.shape[0]
    return pl.pallas_call(
        dispatch_kernel,
        out_shape=jax.ShapeDtypeStruct((pair,) + rows.shape, rows.dtype),
        in_specs=[VMEM_SPEC],
        out_specs=VMEM_SPEC,
        scratch_shapes=[pltpu.SemaphoreType.DMA((groups,))] * 4,
        compiler_params=pltpu.CompilerParams(collective_id=1, has_side_effects=True),
        name="row_dispatch",
    )(rows)


def collect_kernel(parts_ref, out_ref, landed, joined, send_near, recv_near, send_far, recv_far):
    pair, groups = parts_ref.shape[:2]
    group, member = greet_group(groups, pair)
    partner = group * pair + 1 - member
    order = list(range(1, groups)) + [0]
    near = {}
    for step in order:
        target = lax.rem(group + step, groups)
        near[step] = pltpu.make_async_remote_copy(
            src_ref=parts_ref.at[1 - member, target],
            dst_ref=landed.at[target],
            send_sem=send_near.at[step],
            recv_sem=recv_near.at[step],
            device_id={"sp": partner},
            device_id_type=MESH,
        )
        near[step].start()
    far = []
    for step in order:
        target = lax.rem(group + step, groups)
        near[step].wait_recv()
        total = (
            parts_ref[member, target].astype(jnp.float32) + landed[target].astype(jnp.float32)
        ).astype(out_ref.dtype)
        if step == 0:
            out_ref[group] = total
        else:
            joined[target] = total
            copy = pltpu.make_async_remote_copy(
                src_ref=joined.at[target],
                dst_ref=out_ref.at[group],
                send_sem=send_far.at[step],
                recv_sem=recv_far.at[step],
                device_id={"sp": target * pair + member},
                device_id_type=MESH,
            )
            copy.start()
            far.append(copy)
    for step in order:
        near[step].wait_send()
    for copy in far:
        copy.wait()


def collect(parts):
    pair, groups = parts.shape[:2]
    return pl.pallas_call(
        collect_kernel,
        out_shape=jax.ShapeDtypeStruct(parts.shape[1:], parts.dtype),
        in_specs=[VMEM_SPEC],
        out_specs=VMEM_SPEC,
        scratch_shapes=[pltpu.VMEM(parts.shape[1:], parts.dtype)] * 2
        + [pltpu.SemaphoreType.DMA((groups,))] * 4,
        compiler_params=pltpu.CompilerParams(collective_id=2, has_side_effects=True),
        name="row_collect",
    )(parts)


def rotate(payload_tensor, positions):
    channel_dimension = payload_tensor.shape[-1]
    half = channel_dimension // 2
    freq = rope_base ** (-jnp.arange(half, dtype=jnp.float32) * 2.0 / channel_dimension)
    angle = positions.astype(jnp.float32)[:, None, None] * freq[None, None, :]
    cosine = jnp.cos(angle)
    sine = jnp.sin(angle)
    first = payload_tensor[..., :half]
    second = payload_tensor[..., half:]
    return jnp.concatenate([first * cosine - second * sine, first * sine + second * cosine], -1)


def segment_terms(probe_tensor, lookup_tensor, payload_tensor, surge_forgetting, forgetting_speed):
    length = probe_tensor.shape[0]
    segment_tally = jnp.arange(length, dtype=jnp.float32)
    memory_matrix = (
        forgetting_speed[None, :] * segment_tally[:, None] + jnp.cumsum(surge_forgetting)[:, None]
    )
    causal = (segment_tally[:, None] >= segment_tally[None, :])[None]
    level_t = jnp.transpose(memory_matrix)
    gap = level_t[:, :, None] - level_t[:, None, :]
    decay = jnp.where(causal, jnp.exp(jnp.where(causal, gap, 0.0)), 0.0)
    attention_scores = jnp.einsum(
        "szr,yzr->zsy", probe_tensor, lookup_tensor, preferred_element_type=jnp.float32
    )
    weights = (attention_scores * decay).astype(jnp.bfloat16)
    inner = jnp.einsum("htm,mhe->the", weights, payload_tensor, preferred_element_type=jnp.float32)
    factor = jnp.exp(memory_matrix + forgetting_speed[None, :])
    tail = jnp.exp(memory_matrix[-1:, :] - memory_matrix)
    weighted_output = (lookup_tensor.astype(jnp.float32) * tail[:, :, None]).astype(jnp.bfloat16)
    state_update = jnp.einsum(
        "oup,our->upr", weighted_output, payload_tensor, preferred_element_type=jnp.float32
    )
    total = memory_matrix[-1] + forgetting_speed
    return (inner, factor, state_update, total)


def read_state(probe_tensor, state):
    return jnp.einsum(
        "thd,hde->the", probe_tensor.astype(jnp.float32), state, precision=lax.Precision.HIGHEST
    )


def keeping_multiplier(
    probe_source,
    lookup_tensor,
    payload_tensor,
    forgetting_speed,
    surge_forgetting,
    channel_dimension,
    segment_begin,
):
    length = probe_source.shape[0]
    heads = probe_source.shape[1] // channel_dimension
    places = segment_begin + jnp.arange(length, dtype=jnp.int32)
    spun_probe = rotate(
        probe_source.astype(jnp.float32).reshape(length, heads, channel_dimension), places
    ).astype(jnp.bfloat16)
    spun_lookup = (
        rotate(lookup_tensor.astype(jnp.float32).reshape(length, heads, channel_dimension), places)
        * channel_dimension ** (-0.5)
    ).astype(jnp.bfloat16)
    regrouped_payload = payload_tensor.reshape(length, heads, channel_dimension)
    block = min(512, length)
    count = length // block

    def divider_mark(array):
        return array.reshape((count, block) + array.shape[1:])

    state, level, local, reach = None, None, [], []
    for piece in zip(
        divider_mark(spun_probe),
        divider_mark(spun_lookup),
        divider_mark(regrouped_payload),
        divider_mark(surge_forgetting),
    ):
        inner, factor, state_update, total = segment_terms(*piece, forgetting_speed)
        if state is None:
            state, level = state_update, total
        else:
            inner = inner + factor[:, :, None] * read_state(piece[0], state)
            factor = factor * jnp.exp(level)[None, :]
            state, level = jnp.exp(total)[:, None, None] * state + state_update, level + total
        local.append(inner)
        reach.append(factor)
    return (
        spun_probe,
        jnp.concatenate(local, 0),
        jnp.concatenate(reach, 0),
        level,
        state,
    )


def finish(sublayer_final, emission_valve, scaling_coefficients):
    length, heads, channel_dimension = sublayer_final.shape
    normed = sublayer_final * lax.rsqrt(
        jnp.mean(sublayer_final * sublayer_final, -1, keepdims=True) + epsilon
    )
    gated = (
        normed.reshape(length, heads * channel_dimension)
        * scaling_coefficients[None, :]
        * jax.nn.silu(emission_valve.astype(jnp.float32))
    )
    return gated.astype(jnp.bfloat16)


def carried(states, levels):
    place = lax.axis_index("sp")
    count = states.shape[0]
    index = jnp.arange(count, dtype=jnp.int32)
    between = (index[None, :] > index[:, None]) & (index[None, :] < place)
    reach = jnp.sum(jnp.where(between[:, :, None], levels[None, :, :], 0.0), 1)
    weight = jnp.where((index < place)[:, None], jnp.exp(reach), 0.0)
    return jnp.sum(weight[:, :, None, None] * states.astype(jnp.float32), 0)


def slot_positions(chosen, experts, cap):
    listed = chosen.reshape(-1)
    matches = (listed[:, None] == jnp.arange(experts, dtype=jnp.int32)[None, :]).astype(jnp.int32)
    before = jnp.cumsum(matches, 0) - matches
    order = jnp.sum(before * matches, 1)
    return (listed * cap + order).reshape(chosen.shape)


def fill_slots(rows_in, chosen, experts, cap):
    count = rows_in.shape[0]
    places = slot_positions(chosen, experts, cap).reshape(-1)
    owners = jnp.repeat(jnp.arange(count, dtype=jnp.int32), 2)
    source = jnp.full((experts * cap,), count, jnp.int32).at[places].set(owners)
    padded = jnp.concatenate([rows_in, jnp.zeros((1, rows_in.shape[1]), rows_in.dtype)], 0)
    return padded[source].reshape(experts, cap, rows_in.shape[1])


def on_device(
    broad_probe_tensor,
    broad_lookup_tensor,
    broad_payload_tensor,
    broad_emission_valve,
    slim_probe_tensor,
    slim_lookup_tensor,
    slim_payload_tensor,
    slim_emission_valve,
    broad_forgetting_speed,
    slim_forgetting_speed,
    broad_channel_scaling,
    slim_channel_scaling,
    surge_forgetting,
    broad_emission_proj,
    slim_emission_proj,
    skip_stream,
    premix_scaling_coeffs,
    routed_specialist_ids,
    routed_specialist_shares,
    specialist_valve_proj,
    specialist_expand_proj,
    specialist_contract_proj,
):
    length = broad_probe_tensor.shape[0]
    segment_begin = lax.axis_index("sp") * length
    valve_all = lax.all_gather(specialist_valve_proj[0], "tp")
    expand_all = lax.all_gather(specialist_expand_proj[0], "tp")
    contract_all = lax.all_gather(specialist_contract_proj[0], "tp")
    wide_result = keeping_multiplier(
        broad_probe_tensor,
        broad_lookup_tensor,
        broad_payload_tensor,
        broad_forgetting_speed,
        surge_forgetting,
        BROAD_CHANNEL_DIM,
        segment_begin,
    )
    narrow_result = keeping_multiplier(
        slim_probe_tensor,
        slim_lookup_tensor,
        slim_payload_tensor,
        slim_forgetting_speed,
        surge_forgetting,
        THIN_CHANNEL_DIM,
        segment_begin,
    )
    rows = skip_stream.shape[0]
    width = skip_stream.shape[1]
    experts = lax.axis_size("sp") * specialist_valve_proj.shape[0]
    cap = rows * GROUPS // experts
    pair = experts // GROUPS
    own_ids = lax.dynamic_slice_in_dim(routed_specialist_ids, lax.axis_index("tp") * rows, rows, 0)
    own_weights = lax.dynamic_slice_in_dim(
        routed_specialist_shares, lax.axis_index("tp") * rows, rows, 0
    )
    levels = jnp.concatenate([wide_result[3], narrow_result[3]])
    tile = levels
    if pair == 2:
        group_of = own_ids[:, 0] // pair
        named = group_of[:, None] == jnp.arange(GROUPS, dtype=jnp.int32)[None, :]
        rank = jnp.cumsum(named.astype(jnp.int32), 0) - 1
        own_slot = group_of * cap + jnp.sum(jnp.where(named, rank, 0), 1)
        holds = own_slot[None, :] == jnp.arange(GROUPS * cap, dtype=jnp.int32)[:, None]
        member_ids = own_ids - group_of[:, None] * pair
        slot_shares = []
        for member in range(pair):
            share = jnp.sum(jnp.where(member_ids == member, own_weights, 0.0), 1)
            slot_shares.append(jnp.sum(jnp.where(holds, share[None, :], 0.0), 1))
        tile = jnp.concatenate([levels] + slot_shares)
    tile_size = -(-tile.shape[0] // 1024) * 1024
    tile = jnp.pad(tile, (0, tile_size - tile.shape[0])).reshape(-1, 128)
    packed = jnp.concatenate(
        [wide_result[4].reshape(-1, 128), narrow_result[4].reshape(-1, 128)], 0
    ).astype(jnp.bfloat16)
    states, tiles = exchange(packed, tile)
    count = states.shape[0]
    tiles = tiles.reshape(count, -1)
    wide_heads = wide_result[3].shape[0]
    both_heads = levels.shape[0]
    cut = wide_result[4].size // 128
    incoming_wide = carried(
        states[:, :cut].reshape((count,) + wide_result[4].shape), tiles[:, :wide_heads]
    )
    incoming_narrow = carried(
        states[:, cut:].reshape((count,) + narrow_result[4].shape),
        tiles[:, wide_heads:both_heads],
    )
    mixed_wide = finish(
        wide_result[1] + wide_result[2][:, :, None] * read_state(wide_result[0], incoming_wide),
        broad_emission_valve,
        broad_channel_scaling,
    )
    mixed_narrow = finish(
        narrow_result[1] + narrow_result[2][:, :, None] * read_state(narrow_result[0], incoming_narrow),
        slim_emission_valve,
        slim_channel_scaling,
    )
    rows_wide, rows_narrow = (
        lax.all_to_all(mixed_wide, "tp", split_axis=0, concat_axis=1, tiled=True),
        lax.all_to_all(mixed_narrow, "tp", split_axis=0, concat_axis=1, tiled=True),
    )
    projected = jnp.dot(rows_wide, broad_emission_proj, preferred_element_type=jnp.float32)
    projected = projected + jnp.dot(
        rows_narrow, slim_emission_proj, preferred_element_type=jnp.float32
    )
    updated = skip_stream.astype(jnp.float32) + projected
    scale = lax.rsqrt(jnp.mean(updated * updated, -1, keepdims=True) + epsilon)
    normed = (updated * scale * premix_scaling_coeffs[None, :]).astype(jnp.bfloat16)
    if pair == 2:
        spread = holds.astype(jnp.bfloat16)
        filled = jnp.dot(spread, normed, preferred_element_type=jnp.float32).astype(jnp.bfloat16)
        slots = dispatch(filled.reshape(GROUPS, cap, width), pair).reshape(-1, width)
    else:
        own_places = slot_positions(own_ids, experts, cap)
        slots = lax.all_to_all(
            fill_slots(normed, own_ids, experts, cap), "sp", split_axis=0, concat_axis=0, tiled=True
        ).reshape(-1, width)
    expert_out = None
    for part in range(lax.axis_size("tp")):
        emission_valve = jnp.dot(slots, valve_all[part], preferred_element_type=jnp.float32)
        up = jnp.dot(slots, expand_all[part], preferred_element_type=jnp.float32)
        hidden = (jax.nn.silu(emission_valve) * up).astype(jnp.bfloat16)
        term = jnp.dot(hidden, contract_all[part], preferred_element_type=jnp.float32)
        expert_out = term if expert_out is None else expert_out + term
    if pair == 2:
        place = lax.axis_index("sp")
        shares = tiles[:, both_heads : both_heads + pair * GROUPS * cap]
        shares = shares.reshape(GROUPS, pair, pair, GROUPS, cap)
        shares = lax.dynamic_index_in_dim(shares, place % pair, 2, False)
        shares = lax.dynamic_index_in_dim(shares, place // pair, 2, False)
        shares = jnp.transpose(shares, (1, 0, 2)).reshape(-1, 1)
        parts = (expert_out * shares).astype(jnp.bfloat16)
        returned = collect(parts.reshape(pair, GROUPS, cap, width)).reshape(-1, width)
        mixture = lax.dot_general(
            spread, returned, (((0,), (0,)), ((), ())), preferred_element_type=jnp.float32
        )
    else:
        returned = lax.all_to_all(
            expert_out.astype(jnp.bfloat16).reshape(experts, cap, width),
            "sp",
            split_axis=0,
            concat_axis=0,
            tiled=True,
        )
        picked = returned.reshape(experts * cap, width)[own_places]
        mixture = jnp.sum(own_weights[:, :, None] * picked.astype(jnp.float32), 1)
    return (updated + mixture).astype(jnp.bfloat16)


def solution(mesh):
    return jax.shard_map(
        on_device,
        mesh=mesh,
        in_specs=(
            P("sp", "tp"),
            P("sp", "tp"),
            P("sp", "tp"),
            P("sp", "tp"),
            P("sp", "tp"),
            P("sp", "tp"),
            P("sp", "tp"),
            P("sp", "tp"),
            P("tp"),
            P("tp"),
            P("tp"),
            P("tp"),
            P("sp"),
            P(),
            P(),
            P(("sp", "tp"), None),
            P(),
            P("sp", None),
            P("sp", None),
            P("sp", None, "tp"),
            P("sp", None, "tp"),
            P("sp", "tp", None),
        ),
        out_specs=P(("sp", "tp"), None),
        check_vma=False,
    )
```

profile of v0, /device:TPU:0, one launch (start us, length us, event | category | flops | bytes accessed | tf_op | source)
XLA Modules:
  0.0 269.6 jit_solution(15794440631034213515)
XLA Ops:
  6.5 0.7 all-gather.4.cloned.1.call-update
  7.4 0.7 all-gather.6.cloned.1.call-update
  8.1 0.7 all-gather.8.cloned.1.call-update
  8.8 0.3 reduce-window.9
  9.5 0.2 slice_reduce_fusion.2
  9.7 0.6 add.234
  10.5 0.5 add.235
  11.0 0.7 constant_dynamic-slice_fusion.2
  11.7 0.6 multiply_bitcast_fusion
  12.4 0.8 reduce_window_sum.32
  13.5 0.8 copy.161
  14.4 0.2 copy.178
  14.7 0.2 copy.176
  14.9 0.2 copy.177
  15.1 0.2 copy.179
  15.3 1.1 copy.166
  16.4 1.1 copy.160
  17.6 0.3 multiply_cosine_fusion.1
  17.9 0.8 subtract_convert_fusion.1
  18.8 0.7 copy-done.8
  19.6 0.2 convolution_convert_fusion.1
  19.9 0.7 fusion.74
  20.7 1.0 select_reduce_fusion.2
  21.7 0.7 multiply_add_fusion.6
  22.6 1.3 fusion.72.tile_ref
  23.9 1.0 multiply_cosine_fusion
  24.9 0.3 subtract_convert_fusion
  25.2 0.2 fusion.50
  25.7 0.5 convolution_convert_fusion.2
  26.2 0.7 pad_maximum_fusion.5.state_ref
  26.8 21.3 %state_exchange.1 = (bf16[8,384,128]{2,1,0:T(8,128)(2,1)}, f32[8,8,128]{2,1,0:T(8,128)}) custom-call(bf16[384,128]{1,0:T(8,128)(2,1)} %pad_maximum_fusion.5.state_ref, f32[8,128]{1,0:T(8,128)} %fusion.72.tile_ref), custom_call_target="tpu_custom_call" | custom-call | tf_op jit(solution)/shard_map/state_exchange/pallas_call | solution.py:50
  48.1 0.8 copy.193
  49.1 0.2 iota_compare_fusion
  49.4 1.4 multiply_reduce_fusion.1
  50.9 1.2 fusion.23
  52.0 0.6 multiply_reduce_fusion.4
  52.7 0.2 copy.164
  53.0 0.9 fusion.59
  53.9 3.5 %all-to-all-start = ((bf16[4,128,256]{2,1,0:T(8,128)(2,1)}), bf16[4,128,256]{2,1,0:T(8,128)(2,1)S(1)}, u32[]{:S(2)}, u32[]{:S(2)}) async-start(bf16[4,128,256]{2,1,0:T(8,128)(2,1)} %bitcast.18), calls=%async_computation | async-start | bytes 524288 | tf_op jit(solution)/shard_map/all_to_all | solution.py:431
  57.9 0.2 mul.509
  58.1 1.0 multiply_reduce_fusion.3
  59.4 2.1 fusion.24
  61.5 0.5 multiply_reduce_fusion.2
  62.0 0.2 copy.170
  62.4 0.9 fusion.58
  63.3 3.4 %all-to-all-done = bf16[4,128,256]{2,1,0:T(8,128)(2,1)S(1)} async-done(((bf16[4,128,256]{2,1,0:T(8,128)(2,1)}), bf16[4,128,256]{2,1,0:T(8,128)(2,1)S(1)}, u32[]{:S(2)}, u32[]{:S(2)}) %all-to-all-start) | async-done | bytes 262176 | tf_op jit(solution)/shard_map/all_to_all | solution.py:431
  66.6 3.6 %all-to-all-start.1 = ((bf16[4,128,256]{2,1,0:T(8,128)(2,1)}), bf16[4,128,256]{2,1,0:T(8,128)(2,1)S(1)}, u32[]{:S(2)}, u32[]{:S(2)}) async-start(bf16[4,128,256]{2,1,0:T(8,128)(2,1)} %bitcast.25), calls=%async_computation.1 | async-start | bytes 524288 | tf_op jit(solution)/shard_map/all_to_all | solution.py:432
  70.7 5.3 %all-to-all-done.1 = bf16[4,128,256]{2,1,0:T(8,128)(2,1)S(1)} async-done(((bf16[4,128,256]{2,1,0:T(8,128)(2,1)}), bf16[4,128,256]{2,1,0:T(8,128)(2,1)S(1)}, u32[]{:S(2)}, u32[]{:S(2)}) %all-to-all-start.1) | async-done | bytes 262176 | tf_op jit(solution)/shard_map/all_to_all | solution.py:432
  76.2 3.1 %fusion.96 = f32[128,2048]{1,0:T(8,128)S(1)} fusion(bf16[128,1024]{0,1:T(8,128)(2,1)S(1)} %bitcast.178, bf16[1024,2048]{1,0:T(8,128)(2,1)} %param.35), kind=kOutput, calls=%fused_computation.195 | convolution fusion | flops 536870912 | bytes 5505024 | tf_op jit(solution)/shard_map/dot_general | solution.py:434
  79.3 0.3 copy-done.3
  79.8 0.9 multiply_reduce_fusion
  80.7 1.5 convolution_convert_fusion
  82.2 42.8 %row_dispatch.1 = bf16[2,4,64,2048]{3,2,1,0:T(8,128)(2,1)} custom-call(bf16[4,64,2048]{2,1,0:T(8,128)(2,1)} %bitcast.168), custom_call_target="tpu_custom_call" | custom-call | tf_op jit(solution)/shard_map/row_dispatch/pallas_call | solution.py:129
  125.0 4.7 %fusion.3 = f32[512,512]{1,0:T(8,128)} fusion(bf16[512,2048]{1,0:T(8,128)(2,1)} %bitcast.158, bf16[4,2048,512]{2,1,0:T(8,128)(2,1)} %all-gather.4.cloned.1.call-done), kind=kOutput, calls=%fused_computation.11 | convolution fusion | flops 1073741824 | bytes 5242880 | tf_op jit(solution)/shard_map/dot_general | solution.py:452
  129.7 3.9 %fusion.6 = f32[512,512]{1,0:T(8,128)} fusion(bf16[512,2048]{1,0:T(8,128)(2,1)S(1)} %bitcast.159, bf16[4,2048,512]{2,1,0:T(8,128)(2,1)} %all-gather.4.cloned.1.call-done), kind=kOutput, calls=%fused_computation.17 | convolution fusion | flops 1073741824 | bytes 5242880 | tf_op jit(solution)/shard_map/dot_general | solution.py:452
  133.6 2.2 fusion.9
  135.8 2.2 fusion.12
  138.1 54.4 %all-gather.8.cloned.1.call-done = bf16[4,512,2048]{2,1,0:T(8,128)(2,1)} async-done(((bf16[1,512,2048]{2,1,0:T(8,128)(2,1)}), bf16[4,512,2048]{2,1,0:T(8,128)(2,1)}) %all-gather.8.cloned.1.call-update) | async-done | bytes 8388624 | tf_op jit(solution)/shard_map/all_gather | solution.py:360
  192.5 6.9 %fusion.10 = f32[512,2048]{1,0:T(8,128)} fusion(bf16[4,512,2048]{2,1,0:T(8,128)(2,1)} %all-gather.8.cloned.1.call-done, bf16[512,2048]{1,0:T(8,128)(2,1)S(1)} %bitcast.162, bf16[4,2048,512]{2,1,0:T(8,128)(2,1)} %all-gather.6.cloned.1.call-done, f32[512,512]{1,0:T(8,128)} %fusion.12), kind=kOutput, calls=%fused_computation.25 | convolution fusion | flops 2149056512 | bytes 11534336 | tf_op jit(solution)/shard_map/dot_general | solution.py:455
  199.4 7.0 %fusion.7 = f32[512,2048]{1,0:T(8,128)} fusion(bf16[4,512,2048]{2,1,0:T(8,128)(2,1)} %all-gather.8.cloned.1.call-done, bf16[512,2048]{1,0:T(8,128)(2,1)S(1)} %bitcast.163, bf16[4,2048,512]{2,1,0:T(8,128)(2,1)} %all-gather.6.cloned.1.call-done, f32[512,512]{1,0:T(8,128)} %fusion.9), kind=kOutput, calls=%fused_computation.19 | convolution fusion | flops 2149056512 | bytes 11534336 | tf_op jit(solution)/shard_map/dot_general | solution.py:455
  206.4 7.0 %fusion.4 = f32[512,2048]{1,0:T(8,128)} fusion(bf16[4,512,2048]{2,1,0:T(8,128)(2,1)} %all-gather.8.cloned.1.call-done, bf16[512,2048]{1,0:T(8,128)(2,1)S(1)} %bitcast.164, bf16[4,2048,512]{2,1,0:T(8,128)(2,1)} %all-gather.6.cloned.1.call-done, f32[512,512]{1,0:T(8,128)} %fusion.6), kind=kOutput, calls=%fused_computation.13 | convolution fusion | flops 2149056512 | bytes 11534336 | tf_op jit(solution)/shard_map/dot_general | solution.py:455
  213.3 10.1 %multiply_convert_fusion = bf16[512,2048]{1,0:T(8,128)(2,1)} fusion(f32[512,2048]{1,0:T(8,128)} %fusion.4, f32[512,2048]{1,0:T(8,128)} %fusion.10, f32[512,2048]{1,0:T(8,128)} %fusion.7, bf16[4,512,2048]{2,1,0:T(8,128)(2,1)} %all-gather.8.cloned.1.call-done, f32[512]{0:T(512)S(1)} %mul.532, bf16[512,2048]{1,0:T(8,128)(2,1)S(1)} %bitcast.165, ...), kind=kOutput, calls=%fused_computation | convolution fusion | flops 2154299392 | bytes 22022144 | tf_op jit(solution)/shard_map/dot_general | solution.py:455
  223.5 37.2 %row_collect.1 = bf16[4,64,2048]{2,1,0:T(8,128)(2,1)} custom-call(bf16[2,4,64,2048]{3,2,1,0:T(8,128)(2,1)} %bitcast.166), custom_call_target="tpu_custom_call" | custom-call | tf_op jit(solution)/shard_map/row_collect/pallas_call | solution.py:186
  260.7 2.4 fusion.1
  (114 shorter events, 4.1 us)
Async XLA Ops:
  6.5 19.1 %copy-start = (bf16[512,256]{1,0:T(8,128)(2,1)S(1)}, bf16[512,256]{1,0:T(8,128)(2,1)}, u32[]{:S(2)}) copy-start(bf16[512,256]{1,0:T(8,128)(2,1)} %param.24) | copy-start | bytes 786436
  6.5 118.4 %all-gather.4.cloned.1.call-start = ((), (), s32[]{:S(2)}) async-start(), calls=%async_computation.2 | async-start | bytes 10485760 | tf_op jit(solution)/shard_map/all_gather | solution.py:358
  7.3 1.6 copy-start.25
  7.3 2.2 copy-start.18
  7.3 3.0 %copy-start.20 = (f32[4]{0:T(128)S(1)}, f32[4]{0:T(128)}, u32[]{:S(2)}) copy-start(f32[4]{0:T(128)} %param.31) | copy-start | bytes 52
  7.3 5.9 %copy-start.12 = (bf16[512,256]{1,0:T(8,128)(2,1)S(1)}, bf16[512,256]{1,0:T(8,128)(2,1)}, u32[]{:S(2)}) copy-start(bf16[512,256]{1,0:T(8,128)(2,1)} %param.22) | copy-start | bytes 786436
  7.3 6.0 %copy-start.13 = (bf16[512,256]{1,0:T(8,128)(2,1)S(1)}, bf16[512,256]{1,0:T(8,128)(2,1)}, u32[]{:S(2)}) copy-start(bf16[512,256]{1,0:T(8,128)(2,1)} %param.23) | copy-start | bytes 786436
  7.3 130.8 %all-gather.6.cloned.1.call-start = ((), (), s32[]{:S(2)}) async-start(), calls=%async_computation.3 | async-start | bytes 10485760 | tf_op jit(solution)/shard_map/all_gather | solution.py:359
  8.1 5.4 %copy-start.14 = (bf16[512,256]{1,0:T(8,128)(2,1)S(1)}, bf16[512,256]{1,0:T(8,128)(2,1)}, u32[]{:S(2)}) copy-start(bf16[512,256]{1,0:T(8,128)(2,1)} %param.28) | copy-start | bytes 786436
  8.1 184.4 %all-gather.8.cloned.1.call-start = ((), (), s32[]{:S(2)}) async-start(), calls=%async_computation.4 | async-start | bytes 10485760 | tf_op jit(solution)/shard_map/all_gather | solution.py:360
  9.7 2.6 copy-start.29
  11.7 2.9 %copy-start.28 = (s32[128,2]{0,1:T(2,128)}, s32[128,2]{0,1:T(2,128)S(1)}, u32[]{:S(2)}) copy-start(s32[128,2]{0,1:T(2,128)S(1)} %constant_dynamic-slice_fusion.2) | copy-start | bytes 3076
  12.3 2.4 copy-start.24
  17.5 2.1 copy-start.15
  18.8 0.7 copy-start.8
  18.8 0.8 copy-start.10
  22.4 2.8 %copy-start.22 = (s32[128]{0:T(128)}, s32[128]{0:T(128)S(1)}, u32[]{:S(2)}) copy-start(s32[128]{0:T(128)S(1)} %multiply_add_fusion.6) | copy-start | bytes 1540
  24.9 0.7 copy-start.19
  24.9 0.7 copy-start.30
  52.0 1.0 copy-start.6
  52.0 1.0 copy-start.26
  53.9 5.4 %copy-start.21 = (f32[4]{0:T(128)S(1)}, f32[4]{0:T(128)}, u32[]{:S(2)}) copy-start(f32[4]{0:T(128)} %param.31) | copy-start | bytes 52
  53.9 5.5 %copy-start.5 = (bf16[512,4,32]{0,2,1:T(8,128)(2,1)S(1)}, bf16[512,4,32]{0,2,1:T(8,128)(2,1)}, u32[]{:S(2)}) copy-start(bf16[512,4,32]{0,2,1:T(8,128)(2,1)} %get-tuple-element.20) | copy-start | bytes 393220
  53.9 5.5 %copy-start.9 = (f32[512,4,32]{0,2,1:T(8,128)S(1)}, f32[512,4,32]{0,2,1:T(8,128)}, u32[]{:S(2)}) copy-start(f32[512,4,32]{0,2,1:T(8,128)} %copy-done.8) | copy-start | bytes 786436
  53.9 5.5 %copy-start.11 = (f32[512,4,32]{0,2,1:T(8,128)S(1)}, f32[512,4,32]{0,2,1:T(8,128)}, u32[]{:S(2)}) copy-start(f32[512,4,32]{0,2,1:T(8,128)} %copy-done.10) | copy-start | bytes 786436
  53.9 5.5 %copy-start.16 = (bf16[512,256]{0,1:T(8,128)(2,1)S(1)}, bf16[512,256]{0,1:T(8,128)(2,1)}, u32[]{:S(2)}) copy-start(bf16[512,256]{0,1:T(8,128)(2,1)} %copy.161) | copy-start | bytes 786436
  53.9 12.8 %all-to-all-start = ((bf16[4,128,256]{2,1,0:T(8,128)(2,1)}), bf16[4,128,256]{2,1,0:T(8,128)(2,1)S(1)}, u32[]{:S(2)}, u32[]{:S(2)}) async-start(bf16[4,128,256]{2,1,0:T(8,128)(2,1)} %bitcast.18), calls=%async_computation | async-start | bytes 524288 | tf_op jit(solution)/shard_map/all_to_all | solution.py:431
  61.4 1.0 copy-start.7
  61.5 0.9 copy-start.27
  66.6 9.4 %all-to-all-start.1 = ((bf16[4,128,256]{2,1,0:T(8,128)(2,1)}), bf16[4,128,256]{2,1,0:T(8,128)(2,1)S(1)}, u32[]{:S(2)}, u32[]{:S(2)}) async-start(bf16[4,128,256]{2,1,0:T(8,128)(2,1)} %bitcast.25), calls=%async_computation.1 | async-start | bytes 524288 | tf_op jit(solution)/shard_map/all_to_all | solution.py:432
  76.2 3.5 %copy-start.3 = (bf16[1024,2048]{1,0:T(8,128)(2,1)S(1)}, bf16[1024,2048]{1,0:T(8,128)(2,1)}, u32[]{:S(2)}) copy-start(bf16[1024,2048]{1,0:T(8,128)(2,1)} %param.36) | copy-start | bytes 12582916
  76.2 3.6 %copy-start.4 = (bf16[128,2048]{1,0:T(8,128)(2,1)S(1)}, bf16[128,2048]{1,0:T(8,128)(2,1)}, u32[]{:S(2)}) copy-start(bf16[128,2048]{1,0:T(8,128)(2,1)} %param.37) | copy-start | bytes 1572868
  79.8 0.9 copy-start.17
  79.8 0.9 copy-start.23
  124.9 4.7 %copy-start.2 = (bf16[2,4,64,2048]{3,2,1,0:T(8,128)(2,1)S(1)}, bf16[2,4,64,2048]{3,2,1,0:T(8,128)(2,1)}, u32[]{:S(2)}) copy-start(bf16[2,4,64,2048]{3,2,1,0:T(8,128)(2,1)} %row_dispatch.1) | copy-start | bytes 6291460
  125.0 8.6 %copy-start.31 = (bf16[4,2048,512]{2,1,0:T(8,128)(2,1)S(1)}, bf16[4,2048,512]{2,1,0:T(8,128)(2,1)}, u32[]{:S(2)}) copy-start(bf16[4,2048,512]{2,1,0:T(8,128)(2,1)} %all-gather.4.cloned.1.call-done) | copy-start | bytes 25165828
  223.5 39.6 %copy-start.1 = (bf16[512,256]{1,0:T(8,128)(2,1)S(1)}, bf16[512,256]{1,0:T(8,128)(2,1)}, u32[]{:S(2)}) copy-start(bf16[512,256]{1,0:T(8,128)(2,1)} %param.24) | copy-start | bytes 786436
Sparse Core Ops, SparseCore 0:
  8.9 63.8 all-gather.3
  74.3 58.2 all-gather.5
  134.2 58.2 all-gather.7
where the time goes:
time: 270 us
  Pallas kernels  101 us (37%)
  waiting for transfers between devices  65.2 us (24%)
  matrix products  56.9 us (21%)
  other arithmetic  15.4 us (6%)
  between operations  13.7 us (5%)
  local copies, waits for them, and re-layouts  9.94 us (4%)
  starting transfers between devices  7.21 us (3%)
    all_gather x1, waiting for transfers between devices, on_device(): contract_all = lax.all_gather(specialist_contract_proj[0], 'tp')  54.4 us
    pallas_call x1, Pallas kernels, dispatch(): pl.pallas_call(dispatch_kernel, out_shape=jax.ShapeDtypeStruct((pair,) +...  42.8 us
    pallas_call x1, Pallas kernels, collect(): pl.pallas_call(collect_kernel, out_shape=jax.ShapeDtypeStruct(parts.shape...  37.2 us
    dot_general x4, matrix products, on_device(): jnp.dot(hidden, contract_all[part], preferred_element_type=jnp.float32)  31 us
    pallas_call x1, Pallas kernels, exchange(): pl.pallas_call(exchange_kernel, out_shape=(jax.ShapeDtypeStruct((count,)...  21.3 us
    dot_general x4, matrix products, on_device(): jnp.dot(slots, valve_all[part], preferred_element_type=jnp.float32)  13.1 us
  transfers between devices with their start and end apart: 5, of which 3 were waited for; matrix products, arithmetic and copies ran while one was open for 17% of the time, Pallas kernels for 24%

commit v1 on v0

--- a/solution.py
+++ b/solution.py
@@ -64,135 +64,272 @@
     )(state, tile)
 
 
-def greet_group(groups, pair):
-    me = lax.axis_index("sp")
-    group = me // pair
-    member = lax.rem(me, pair)
+def places_of(groups):
+    sp = lax.axis_index("sp")
+    tp = lax.axis_index("tp")
+    core = lax.rem(tp, 2)
+    x = lax.rem(sp, 2)
+    y = tp // 2
+    across_sp = sp + 1 - 2 * x
+    across_tp = tp + 2 - 4 * y
+    near = {"sp": across_sp + core * (sp - across_sp), "tp": tp + core * (across_tp - tp)}
+    side = {"sp": sp + core * (across_sp - sp), "tp": across_tp + core * (tp - across_tp)}
+    twin = {"sp": sp, "tp": tp + 1 - 2 * core}
+    group = sp // 2
+    far = [{"sp": lax.rem(group + step, groups) * 2 + x, "tp": tp} for step in range(groups)]
+    return group, x, y, core, near, side, twin, far
+
+
+def experts_kernel(
+    rows_ref,
+    shares_ref,
+    valve_ref,
+    expand_ref,
+    contract_ref,
+    out_ref,
+    slots,
+    valve,
+    expand,
+    contract,
+    hidden,
+    kept,
+    leave,
+    landed,
+    joined,
+    met,
+    back,
+    load_sem,
+    swap_send,
+    swap_recv,
+    far_send,
+    far_recv,
+    near_send,
+    near_recv,
+    fold_send,
+    fold_recv,
+    home_send,
+    home_recv,
+):
+    groups, cap, width = rows_ref.shape
+    units = valve_ref.shape[1]
+    group, x, y, core, near, side, twin, far = places_of(groups)
     barrier = pltpu.get_barrier_semaphore()
-    for step in range(1, groups):
-        pl.semaphore_signal(
-            barrier,
-            inc=1,
-            device_id={"sp": lax.rem(group + step, groups) * pair + member},
+    friends = [near, side, twin] + far[1:]
+    for friend in friends:
+        pl.semaphore_signal(barrier, inc=1, device_id=friend, device_id_type=MESH)
+    pl.semaphore_wait(barrier, len(friends))
+    sent = []
+
+    def send(src, dst, send_sem, recv_sem, device):
+        copy = pltpu.make_async_remote_copy(
+            src_ref=src,
+            dst_ref=dst,
+            send_sem=send_sem,
+            recv_sem=recv_sem,
+            device_id=device,
             device_id_type=MESH,
         )
-    pl.semaphore_signal(
-        barrier, inc=1, device_id={"sp": group * pair + 1 - member}, device_id_type=MESH
-    )
-    pl.semaphore_wait(barrier, groups)
-    return group, member
-
-
-def dispatch_kernel(rows_ref, out_ref, send_far, recv_far, send_near, recv_near):
-    groups = rows_ref.shape[0]
-    pair = out_ref.shape[0]
-    group, member = greet_group(groups, pair)
-    partner = group * pair + 1 - member
-    far = []
-    for step in range(1, groups):
-        target = lax.rem(group + step, groups)
-        copy = pltpu.make_async_remote_copy(
-            src_ref=rows_ref.at[target],
-            dst_ref=out_ref.at[member, group],
-            send_sem=send_far.at[step],
-            recv_sem=recv_far.at[step],
-            device_id={"sp": target * pair + member},
-            device_id_type=MESH,
-        )
         copy.start()
-        far.append(copy)
-    near = []
-    for step in range(groups):
-        origin = lax.rem(group - step + groups, groups)
+        sent.append(copy)
+        return copy
+
+    order = [0, 1, 3, 2]
+    arriving = {}
+    for step in order[1:]:
+        arriving[step] = send(
+            rows_ref.at[lax.rem(group + step, groups)],
+            slots.at[step, 0],
+            far_send.at[step],
+            far_recv.at[step],
+            far[step],
+        )
+    own = {}
+
+    def spread(step):
         if step > 0:
-            far[step - 1].wait_recv()
-        copy = pltpu.make_async_remote_copy(
-            src_ref=rows_ref.at[group] if step == 0 else out_ref.at[member, origin],
-            dst_ref=out_ref.at[member, origin],
-            send_sem=send_near.at[step],
-            recv_sem=recv_near.at[step],
-            device_id={"sp": partner},
-            device_id_type=MESH,
-        )
-        copy.start()
-        near.append(copy)
-        if step == 0:
-            out_ref[member, group] = rows_ref[group]
-    for copy in far:
-        copy.wait_send()
-    for copy in near:
-        copy.wait()
-
-
-def dispatch(rows, pair):
-    groups = rows.shape[0]
-    return pl.pallas_call(
-        dispatch_kernel,
-        out_shape=jax.ShapeDtypeStruct((pair,) + rows.shape, rows.dtype),
-        in_specs=[VMEM_SPEC],
-        out_specs=VMEM_SPEC,
-        scratch_shapes=[pltpu.SemaphoreType.DMA((groups,))] * 4,
-        compiler_params=pltpu.CompilerParams(collective_id=1, has_side_effects=True),
-        name="row_dispatch",
-    )(rows)
-
-
-def collect_kernel(parts_ref, out_ref, landed, joined, send_near, recv_near, send_far, recv_far):
-    pair, groups = parts_ref.shape[:2]
-    group, member = greet_group(groups, pair)
-    partner = group * pair + 1 - member
-    order = list(range(1, groups)) + [0]
-    near = {}
-    for step in order:
-        target = lax.rem(group + step, groups)
-        near[step] = pltpu.make_async_remote_copy(
-            src_ref=parts_ref.at[1 - member, target],
-            dst_ref=landed.at[target],
-            send_sem=send_near.at[step],
-            recv_sem=recv_near.at[step],
-            device_id={"sp": partner},
-            device_id_type=MESH,
-        )
-        near[step].start()
-    far = []
-    for step in order:
-        target = lax.rem(group + step, groups)
-        near[step].wait_recv()
-        total = (
-            parts_ref[member, target].astype(jnp.float32) + landed[target].astype(jnp.float32)
-        ).astype(out_ref.dtype)
+            arriving[step].wait_recv()
+        src = rows_ref.at[group] if step == 0 else slots.at[step, 0]
+        own[step] = [
+            send(src, slots.at[step, 1], near_send.at[step, 0], near_recv.at[step, 0], near),
+            send(src, slots.at[step, 2], near_send.at[step, 1], near_recv.at[step, 1], side),
+        ]
+
+    def forward(step):
+        own[step][0].wait_recv()
+        own[step].append(
+            send(
+                slots.at[step, 1],
+                slots.at[step, 3],
+                near_send.at[step, 2],
+                near_recv.at[step, 2],
+                side,
+            )
+        )
+
+    spread(0)
+    loads = []
+    swaps = []
+    for index, (src, dst) in enumerate(
+        ((valve_ref, valve), (expand_ref, expand), (contract_ref, contract))
+    ):
+        load = pltpu.make_async_copy(src, dst.at[core], load_sem.at[index])
+        load.start()
+        loads.append(load)
+        swaps.append(send(src, dst.at[core], swap_send.at[index], swap_recv.at[index], twin))
+    slots[0, 0] = rows_ref[group]
+    forward(0)
+    spread(order[1])
+
+    def shares_for(step):
+        origin = lax.rem(group + groups - step, groups)
+        near_x = 1 - x + core * (2 * x - 1)
+        near_y = y + core * (1 - 2 * y)
+        return jnp.concatenate(
+            [
+                shares_ref[origin, x, y],
+                shares_ref[origin, near_x, near_y],
+                shares_ref[origin, 1 - near_x + 0 * x, 1 - near_y],
+                shares_ref[origin, 1 - x, 1 - y],
+            ],
+            0,
+        )
+
+    tile = 256
+    across = 512
+
+    def widen(step):
+        share = shares_for(step)
+        batch = slots[step].reshape(4 * cap, width)
+
+        def one(index, carry):
+            half = index // (units // tile)
+            begin = pl.multiple_of(lax.rem(index, units // tile) * tile, tile)
+            gate = jnp.dot(
+                batch, valve[half, :, pl.ds(begin, tile)], preferred_element_type=jnp.float32
+            )
+            up = jnp.dot(
+                batch, expand[half, :, pl.ds(begin, tile)], preferred_element_type=jnp.float32
+            )
+            place = pl.multiple_of(index * tile, tile)
+            hidden[:, pl.ds(place, tile)] = (jax.nn.silu(gate) * up * share).astype(hidden.dtype)
+            return carry
+
+        lax.fori_loop(0, 2 * units // tile, one, 0)
+
+    def narrow(step):
+        def one(index, carry):
+            begin = pl.multiple_of(index * across, across)
+            column = pl.ds(begin, across)
+            part = jnp.dot(
+                hidden[:, :units], contract[0, :, column], preferred_element_type=jnp.float32
+            ) + jnp.dot(
+                hidden[:, units:], contract[1, :, column], preferred_element_type=jnp.float32
+            )
+            kept[step, :, :, column] = part[: 2 * cap].reshape(2, cap, across)
+            leave[step, :, :, column] = part[2 * cap :].reshape(2, cap, across).astype(leave.dtype)
+            return carry
+
+        lax.fori_loop(0, width // across, one, 0)
+        folding[step] = send(
+            leave.at[step], landed.at[step], fold_send.at[step, 0], fold_recv.at[step, 0], side
+        )
+
+    folding = {}
+    joining = {}
+
+    def join(step):
+        folding[step].wait_recv()
+        joined[step] = (kept[step, 1] + landed[step, 1].astype(jnp.float32)).astype(joined.dtype)
+        joining[step] = send(
+            joined.at[step], met.at[step], fold_send.at[step, 1], fold_recv.at[step, 1], near
+        )
+        kept[step, 0] = kept[step, 0] + landed[step, 0].astype(jnp.float32)
+
+    homing = []
+
+    def finish_step(step):
+        joining[step].wait_recv()
+        total = (kept[step, 0] + met[step].astype(jnp.float32)).astype(out_ref.dtype)
         if step == 0:
             out_ref[group] = total
         else:
-            joined[target] = total
-            copy = pltpu.make_async_remote_copy(
-                src_ref=joined.at[target],
-                dst_ref=out_ref.at[group],
-                send_sem=send_far.at[step],
-                recv_sem=recv_far.at[step],
-                device_id={"sp": target * pair + member},
-                device_id_type=MESH,
+            back[step] = total
+            homing.append(
+                send(
+                    back.at[step],
+                    out_ref.at[group],
+                    home_send.at[step],
+                    home_recv.at[step],
+                    far[groups - step],
+                )
             )
-            copy.start()
-            far.append(copy)
-    for step in order:
-        near[step].wait_send()
-    for copy in far:
-        copy.wait()
-
-
-def collect(parts):
-    pair, groups = parts.shape[:2]
+
+    for place, step in enumerate(order):
+        own[step][1].wait_recv()
+        own[step][2].wait_recv()
+        if place == 0:
+            for load, swap in zip(loads, swaps):
+                load.wait()
+                swap.wait_recv()
+        widen(step)
+        if place + 1 < groups:
+            forward(order[place + 1])
+        if place + 2 < groups:
+            spread(order[place + 2])
+        narrow(step)
+        if place >= 1:
+            join(order[place - 1])
+        if place >= 2:
+            finish_step(order[place - 2])
+    join(order[-1])
+    finish_step(order[-2])
+    finish_step(order[-1])
+    for copy in homing:
+        copy.wait_recv()
+    for copy in sent:
+        copy.wait_send()
+
+
+def experts_plane(rows, shares, valve, expand, contract):
+    groups, cap, width = rows.shape
+    units = valve.shape[1]
+    kind = rows.dtype
+    any_spec = pl.BlockSpec(memory_space=pl.ANY)
+    dma = pltpu.SemaphoreType.DMA
     return pl.pallas_call(
-        collect_kernel,
-        out_shape=jax.ShapeDtypeStruct(parts.shape[1:], parts.dtype),
-        in_specs=[VMEM_SPEC],
+        experts_kernel,
+        out_shape=jax.ShapeDtypeStruct(rows.shape, kind),
+        in_specs=[VMEM_SPEC] * 2 + [any_spec] * 3,
         out_specs=VMEM_SPEC,
-        scratch_shapes=[pltpu.VMEM(parts.shape[1:], parts.dtype)] * 2
-        + [pltpu.SemaphoreType.DMA((groups,))] * 4,
-        compiler_params=pltpu.CompilerParams(collective_id=2, has_side_effects=True),
-        name="row_collect",
-    )(parts)
+        scratch_shapes=[
+            pltpu.VMEM((groups, 4, cap, width), kind),
+            pltpu.VMEM((2,) + valve.shape, kind),
+            pltpu.VMEM((2,) + expand.shape, kind),
+            pltpu.VMEM((2,) + contract.shape, kind),
+            pltpu.VMEM((4 * cap, 2 * units), kind),
+            pltpu.VMEM((groups, 2, cap, width), jnp.float32),
+            pltpu.VMEM((groups, 2, cap, width), kind),
+            pltpu.VMEM((groups, 2, cap, width), kind),
+            pltpu.VMEM((groups, cap, width), kind),
+            pltpu.VMEM((groups, cap, width), kind),
+            pltpu.VMEM((groups, cap, width), kind),
+            dma((3,)),
+            dma((3,)),
+            dma((3,)),
+            dma((groups,)),
+            dma((groups,)),
+            dma((groups, 3)),
+            dma((groups, 3)),
+            dma((groups, 2)),
+            dma((groups, 2)),
+            dma((groups,)),
+            dma((groups,)),
+        ],
+        compiler_params=pltpu.CompilerParams(
+            collective_id=3, has_side_effects=True, vmem_limit_bytes=56 * 1024 * 1024
+        ),
+        name="experts_plane",
+    )(rows, shares, valve, expand, contract)
 
 
 def rotate(payload_tensor, positions):
@@ -327,6 +464,22 @@
     source = jnp.full((experts * cap,), count, jnp.int32).at[places].set(owners)
     padded = jnp.concatenate([rows_in, jnp.zeros((1, rows_in.shape[1]), rows_in.dtype)], 0)
     return padded[source].reshape(experts, cap, rows_in.shape[1])
+
+
+def shares_by_slot(ids, shares, rows, cap):
+    core = lax.rem(lax.axis_index("tp"), 2)
+    ids = lax.dynamic_index_in_dim(ids.reshape(-1, 2, rows, 2), core, 1, False)
+    shares = lax.dynamic_index_in_dim(shares.reshape(-1, 2, rows, 2), core, 1, False)
+    group = ids[:, :, 0] // 2
+    named = group[:, :, None] == jnp.arange(GROUPS, dtype=jnp.int32)
+    rank = jnp.cumsum(named.astype(jnp.int32), 1) - 1
+    slot = group * cap + jnp.sum(jnp.where(named, rank, 0), 2)
+    holds = slot[:, None, :] == jnp.arange(GROUPS * cap, dtype=jnp.int32)[None, :, None]
+    found = []
+    for member in range(2):
+        share = jnp.sum(jnp.where(ids - 2 * group[:, :, None] == member, shares, 0.0), 2)
+        found.append(jnp.sum(jnp.where(holds, share[:, None, :], 0.0), 2))
+    return jnp.stack(found, 1).reshape(-1)
 
 
 def on_device(
@@ -355,9 +508,13 @@
 ):
     length = broad_probe_tensor.shape[0]
     segment_begin = lax.axis_index("sp") * length
-    valve_all = lax.all_gather(specialist_valve_proj[0], "tp")
-    expand_all = lax.all_gather(specialist_expand_proj[0], "tp")
-    contract_all = lax.all_gather(specialist_contract_proj[0], "tp")
+    plane = lax.axis_size("sp") * specialist_valve_proj.shape[0] == 2 * GROUPS and (
+        lax.axis_size("tp") == 4
+    )
+    if not plane:
+        valve_all = lax.all_gather(specialist_valve_proj[0], "tp")
+        expand_all = lax.all_gather(specialist_expand_proj[0], "tp")
+        contract_all = lax.all_gather(specialist_contract_proj[0], "tp")
     wide_result = keeping_multiplier(
         broad_probe_tensor,
         broad_lookup_tensor,
@@ -387,18 +544,15 @@
     )
     levels = jnp.concatenate([wide_result[3], narrow_result[3]])
     tile = levels
-    if pair == 2:
+    if plane:
         group_of = own_ids[:, 0] // pair
         named = group_of[:, None] == jnp.arange(GROUPS, dtype=jnp.int32)[None, :]
         rank = jnp.cumsum(named.astype(jnp.int32), 0) - 1
         own_slot = group_of * cap + jnp.sum(jnp.where(named, rank, 0), 1)
         holds = own_slot[None, :] == jnp.arange(GROUPS * cap, dtype=jnp.int32)[:, None]
-        member_ids = own_ids - group_of[:, None] * pair
-        slot_shares = []
-        for member in range(pair):
-            share = jnp.sum(jnp.where(member_ids == member, own_weights, 0.0), 1)
-            slot_shares.append(jnp.sum(jnp.where(holds, share[None, :], 0.0), 1))
-        tile = jnp.concatenate([levels] + slot_shares)
+        tile = jnp.concatenate(
+            [levels, shares_by_slot(routed_specialist_ids, routed_specialist_shares, rows, cap)]
+        )
     tile_size = -(-tile.shape[0] // 1024) * 1024
     tile = jnp.pad(tile, (0, tile_size - tile.shape[0])).reshape(-1, 128)
     packed = jnp.concatenate(
@@ -438,15 +592,29 @@
     updated = skip_stream.astype(jnp.float32) + projected
     scale = lax.rsqrt(jnp.mean(updated * updated, -1, keepdims=True) + epsilon)
     normed = (updated * scale * premix_scaling_coeffs[None, :]).astype(jnp.bfloat16)
-    if pair == 2:
+    if plane:
         spread = holds.astype(jnp.bfloat16)
         filled = jnp.dot(spread, normed, preferred_element_type=jnp.float32).astype(jnp.bfloat16)
-        slots = dispatch(filled.reshape(GROUPS, cap, width), pair).reshape(-1, width)
-    else:
-        own_places = slot_positions(own_ids, experts, cap)
-        slots = lax.all_to_all(
-            fill_slots(normed, own_ids, experts, cap), "sp", split_axis=0, concat_axis=0, tiled=True
+        shares = tiles[:, both_heads : both_heads + 4 * GROUPS * cap]
+        shares = shares.reshape(GROUPS, 2, 2, 2, GROUPS, cap)
+        place = lax.axis_index("sp")
+        shares = lax.dynamic_index_in_dim(shares, place % 2, 3, False)
+        shares = lax.dynamic_index_in_dim(shares, place // 2, 3, False)
+        returned = experts_plane(
+            filled.reshape(GROUPS, cap, width),
+            shares[..., None],
+            specialist_valve_proj[0],
+            specialist_expand_proj[0],
+            specialist_contract_proj[0],
         ).reshape(-1, width)
+        mixture = lax.dot_general(
+            spread, returned, (((0,), (0,)), ((), ())), preferred_element_type=jnp.float32
+        )
+        return (updated + mixture).astype(jnp.bfloat16)
+    own_places = slot_positions(own_ids, experts, cap)
+    slots = lax.all_to_all(
+        fill_slots(normed, own_ids, experts, cap), "sp", split_axis=0, concat_axis=0, tiled=True
+    ).reshape(-1, width)
     expert_out = None
     for part in range(lax.axis_size("tp")):
         emission_valve = jnp.dot(slots, valve_all[part], preferred_element_type=jnp.float32)
@@ -454,28 +622,15 @@
         hidden = (jax.nn.silu(emission_valve) * up).astype(jnp.bfloat16)
         term = jnp.dot(hidden, contract_all[part], preferred_element_type=jnp.float32)
         expert_out = term if expert_out is None else expert_out + term
-    if pair == 2:
-        place = lax.axis_index("sp")
-        shares = tiles[:, both_heads : both_heads + pair * GROUPS * cap]
-        shares = shares.reshape(GROUPS, pair, pair, GROUPS, cap)
-        shares = lax.dynamic_index_in_dim(shares, place % pair, 2, False)
-        shares = lax.dynamic_index_in_dim(shares, place // pair, 2, False)
-        shares = jnp.transpose(shares, (1, 0, 2)).reshape(-1, 1)
-        parts = (expert_out * shares).astype(jnp.bfloat16)
-        returned = collect(parts.reshape(pair, GROUPS, cap, width)).reshape(-1, width)
-        mixture = lax.dot_general(
-            spread, returned, (((0,), (0,)), ((), ())), preferred_element_type=jnp.float32
-        )
-    else:
-        returned = lax.all_to_all(
-            expert_out.astype(jnp.bfloat16).reshape(experts, cap, width),
-            "sp",
-            split_axis=0,
-            concat_axis=0,
-            tiled=True,
-        )
-        picked = returned.reshape(experts * cap, width)[own_places]
-        mixture = jnp.sum(own_weights[:, :, None] * picked.astype(jnp.float32), 1)
+    returned = lax.all_to_all(
+        expert_out.astype(jnp.bfloat16).reshape(experts, cap, width),
+        "sp",
+        split_axis=0,
+        concat_axis=0,
+        tiled=True,
+    )
+    picked = returned.reshape(experts * cap, width)[own_places]
+    mixture = jnp.sum(own_weights[:, :, None] * picked.astype(jnp.float32), 1)
     return (updated + mixture).astype(jnp.bfloat16)
 
 

time: 270 us -> 189 us (0.70)
  waiting for transfers between devices: 65.2 us -> 5.74 us
  matrix products: 56.9 us -> 15.7 us
  Pallas kernels: 101 us -> 121 us
  between operations: 13.7 us -> 0.62 us
  other arithmetic: 15.4 us -> 22.9 us
  local copies, waits for them, and re-layouts: 9.94 us -> 14.2 us
    all_gather x3 -> x0, waiting for transfers between devices: 54.4 us -> none  [the longest x1 54.4 us: on_device(): contract_all = lax.all_gather(specialist_contract_proj[0], 'tp')]
    dot_general x8 -> x0, matrix products: 44.1 us -> none  [the longest x4 31 us: on_device(): jnp.dot(hidden, contract_all[part], preferred_element_type=jnp.float32)]
    pallas_call x2 -> x1, Pallas kernels: 80 us -> 99.2 us  [experts_plane(): pl.pallas_call(experts_kernel, out_shape=jax.ShapeDtypeStruct(rows.shape,...]
    all_to_all x1, waiting for transfers between devices: 3.37 us -> 0.01 us  [on_device(): lax.all_to_all(mixed_wide, 'tp', split_axis=0, concat_axis=1, tiled=True)]
    another operation x5 -> x7, other arithmetic: 1.54 us -> 4.29 us
    unnamed x73 -> x49, local copies, waits for them, and re-layouts: 4.49 us -> 5.94 us
  transfers between devices with their start and end apart: 5 -> 2, of which waited for: 3 -> 1; matrix products, arithmetic and copies ran while one was open for 17% -> 5% of each run, Pallas kernels for 24% -> 0%
where the time goes in v1:
time: 189 us; the launch traced here: 187 us
  Pallas kernels  121 us (64%)
  other arithmetic  22.9 us (12%)
  matrix products  15.7 us (8%)
  local copies, waits for them, and re-layouts  14.2 us (8%)
  starting transfers between devices  6.99 us (4%)
  waiting for transfers between devices  5.74 us (3%)
    pallas_call x1, Pallas kernels, experts_plane(): pl.pallas_call(experts_kernel, out_shape=jax.ShapeDtypeStruct(rows.shape,...  99.2 us
    pallas_call x1, Pallas kernels, exchange(): pl.pallas_call(exchange_kernel, out_shape=(jax.ShapeDtypeStruct((count,)...  21.8 us
    unnamed x49, local copies, waits for them, and re-layouts  5.94 us
    all_to_all x1, waiting for transfers between devices, on_device(): lax.all_to_all(mixed_narrow, 'tp', split_axis=0, concat_axis=1, tiled=True)  5.74 us
    dot_general x2, matrix products, segment_terms(): jnp.einsum('htm,mhe->the', weights, payload_tensor, preferred_element_typ...  5.19 us
    another operation x5, other arithmetic  4.09 us
  transfers between devices with their start and end apart: 2, of which 1 were waited for; matrix products, arithmetic and copies ran while one was open for 5% of the time, Pallas kernels for 0%

profile of v1, /device:TPU:0, one launch (start us, length us, event | category | flops | bytes accessed | tf_op | source)
XLA Modules:
  0.0 187.2 jit_solution(15915521839309128399)
XLA Ops:
  0.0 0.9 iota_compare_fusion
  1.0 1.0 reduce-window.9
  2.2 1.3 multiply_add_fusion.5
  3.6 0.7 multiply_add_fusion.4
  4.3 0.2 slice_reduce_fusion.2
  4.5 1.3 add_exponential_fusion.1
  5.8 1.2 add.232
  7.0 0.7 multiply_add_fusion.3
  7.8 0.2 slice_reduce_fusion
  7.9 1.3 add_exponential_fusion
  9.3 1.2 add.233
  10.5 1.1 copy.130
  11.7 0.2 copy.157
  11.9 0.2 copy.156
  12.1 0.6 iota_compare_fusion.8
  12.7 1.1 copy.133
  13.8 0.2 copy.159
  14.0 0.2 copy.158
  14.2 0.9 copy.140
  15.2 1.8 multiply_cosine_fusion
  17.1 1.0 multiply_cosine_fusion.1
  18.0 1.1 copy.139
  19.1 1.7 subtract_convert_fusion.1
  20.8 0.7 copy-done.7
  21.7 1.2 convolution_convert_fusion.1
  22.9 0.7 reshape.714
  23.6 0.7 reshape.713
  24.5 0.2 reduce_window_sum.43
  24.7 0.2 select_reduce_fusion.2
  24.9 0.2 select_reduce_fusion.1
  25.2 0.8 concatenate.25
  25.9 0.6 pad_bitcast_fusion.tile_ref
  26.5 1.3 subtract_convert_fusion
  27.8 0.2 fusion.22
  28.1 0.5 convolution_convert_fusion.2
  28.6 0.6 pad_maximum_fusion.5.state_ref
  29.2 21.8 %state_exchange.1 = (bf16[8,384,128]{2,1,0:T(8,128)(2,1)}, f32[8,16,128]{2,1,0:T(8,128)}) custom-call(bf16[384,128]{1,0:T(8,128)(2,1)} %pad_maximum_fusion.5.state_ref, f32[16,128]{1,0:T(8,128)} %pad_bitcast_fusion.tile_ref), custom_call_target="tpu_custom_call" | custom-call | tf_op jit(solution)/shard_map/state_exchange/pallas_call | solution.py:50
  51.0 0.9 copy.173
  52.2 1.4 multiply_reduce_fusion.1
  53.6 2.1 %fusion.4 = f32[512,2,128]{0,2,1:T(8,128)S(1)} fusion(bf16[512,2,128]{2,0,1:T(8,128)(2,1)S(1)} %fusion.22, f32[2,512]{1,0:T(2,128)} %multiply_add_fusion.5, pred[512,512]{1,0:T(8,128)(4,1)} %iota_compare_fusion, bf16[512,2,64]{2,0,1:T(8,128)(2,1)S(1)} %get-tuple-element.16, bf16[512,2,64]{2,0,1:T(8,128)(2,1)S(1)} %get-tuple-element.15, ...), kind=kOutput, calls=%fused_computation.9 | convolution fusion | flops 271581184 | bytes 1576960 | tf_op jit(solution)/shard_map/htm,mhe->the/dot_general | solution.py:361
  55.8 0.6 multiply_reduce_fusion.4
  56.4 0.2 copy.144
  56.7 0.9 fusion.27
  57.6 3.4 %all-to-all-start = ((bf16[4,128,256]{2,1,0:T(8,128)(2,1)}), bf16[4,128,256]{2,1,0:T(8,128)(2,1)S(1)}, u32[]{:S(2)}, u32[]{:S(2)}) async-start(bf16[4,128,256]{2,1,0:T(8,128)(2,1)} %bitcast.22), calls=%async_computation | async-start | bytes 524288 | tf_op jit(solution)/shard_map/all_to_all | solution.py:585
  61.6 0.2 mul.479
  61.8 1.0 multiply_reduce_fusion.3
  63.0 3.0 %fusion.5 = f32[512,4,64]{0,2,1:T(8,128)S(1)} fusion(bf16[512,4,64]{0,2,1:T(8,128)(2,1)} %bitcast.128, f32[4,512]{1,0:T(4,128)S(1)} %multiply_add_fusion.2, pred[512,512]{1,0:T(8,128)(4,1)S(1)} %copy-done.12, bf16[512,4,32]{0,2,1:T(8,128)(2,1)S(1)} %copy-done.3, bf16[512,4,32]{0,2,1:T(8,128)(2,1)S(1)} %get-tuple-element.19, ...), kind=kOutput, calls=%fused_computation.10 | convolution fusion | flops 274595840 | bytes 1843200 | tf_op jit(solution)/shard_map/htm,mhe->the/dot_general | solution.py:361
  66.0 0.5 multiply_reduce_fusion.2
  66.6 0.2 copy.150
  66.8 0.7 constant_dynamic-slice_fusion
  67.6 0.2 reduce_window_sum.44
  67.8 0.2 select_reduce_fusion.3
  68.1 1.0 copy.152.shares_ref
  69.2 0.9 fusion.26
  70.0 3.6 %all-to-all-start.1 = ((bf16[4,128,256]{2,1,0:T(8,128)(2,1)}), bf16[4,128,256]{2,1,0:T(8,128)(2,1)S(1)}, u32[]{:S(2)}, u32[]{:S(2)}) async-start(bf16[4,128,256]{2,1,0:T(8,128)(2,1)} %bitcast.29), calls=%async_computation.1 | async-start | bytes 524288 | tf_op jit(solution)/shard_map/all_to_all | solution.py:586
  73.6 0.2 copy.145
  73.8 5.7 %all-to-all-done.1 = bf16[4,128,256]{2,1,0:T(8,128)(2,1)S(1)} async-done(((bf16[4,128,256]{2,1,0:T(8,128)(2,1)}), bf16[4,128,256]{2,1,0:T(8,128)(2,1)S(1)}, u32[]{:S(2)}, u32[]{:S(2)}) %all-to-all-start.1) | async-done | bytes 262176 | tf_op jit(solution)/shard_map/all_to_all | solution.py:586
  79.5 0.2 copy.151
  79.7 3.1 %fusion.61 = f32[128,2048]{1,0:T(8,128)S(1)} fusion(bf16[128,1024]{0,1:T(8,128)(2,1)S(1)} %bitcast.125, bf16[1024,2048]{1,0:T(8,128)(2,1)} %param.35), kind=kOutput, calls=%fused_computation.159 | convolution fusion | flops 536870912 | bytes 5505024 | tf_op jit(solution)/shard_map/dot_general | solution.py:588
  82.8 0.3 copy-done.1
  83.2 0.9 multiply_reduce_fusion
  84.0 1.5 convolution_convert_fusion
  85.5 99.2 %experts_plane.1 = bf16[4,64,2048]{2,1,0:T(8,128)(2,1)} custom-call(bf16[4,64,2048]{2,1,0:T(8,128)(2,1)} %bitcast.112, f32[4,2,2,64,1]{4,3,2,1,0:T(8,128)} %copy.152.shares_ref, bf16[2048,512]{1,0:T(8,128)(2,1)} %bitcast.115, bf16[2048,512]{1,0:T(8,128)(2,1)} %bitcast.116, bf16[512,2048]{1,0:T(8,128)(2,1)} %bitcast.117), custom_call_target="tpu_custom_call" | custom-call | tf_op jit(solution)/shard_map/experts_plane/pallas_call | solution.py:299
  184.8 2.4 %fusion.1 = bf16[128,2048]{1,0:T(8,128)(2,1)} fusion(f32[128,2048]{1,0:T(8,128)S(1)} %get-tuple-element.44, bf16[256,2048]{1,0:T(8,128)(2,1)} %bitcast.111, s32[128]{0:T(128)S(1)} %multiply_add_fusion.7), kind=kOutput, calls=%fused_computation.5 | convolution fusion | flops 134774784 | bytes 2621952 | tf_op jit(solution)/shard_map/dot_general | solution.py:610
  (84 shorter events, 2.3 us)
Async XLA Ops:
  0.0 28.1 %copy-start = (bf16[512,256]{1,0:T(8,128)(2,1)S(1)}, bf16[512,256]{1,0:T(8,128)(2,1)}, u32[]{:S(2)}) copy-start(bf16[512,256]{1,0:T(8,128)(2,1)} %param.24) | copy-start | bytes 786436
  0.0 14.2 %copy-start.11 = (bf16[512,256]{1,0:T(8,128)(2,1)S(1)}, bf16[512,256]{1,0:T(8,128)(2,1)}, u32[]{:S(2)}) copy-start(bf16[512,256]{1,0:T(8,128)(2,1)} %param.28) | copy-start | bytes 786436
  0.0 15.1 %copy-start.4 = (bf16[512,256]{1,0:T(8,128)(2,1)S(1)}, bf16[512,256]{1,0:T(8,128)(2,1)}, u32[]{:S(2)}) copy-start(bf16[512,256]{1,0:T(8,128)(2,1)} %param.26) | copy-start | bytes 786436
  20.8 0.7 copy-start.7
  20.8 0.8 copy-start.9
  20.8 7.2 %copy-start.15 = (f32[512,2]{0,1:T(2,128)S(1)}, f32[512,2]{0,1:T(2,128)}, u32[]{:S(2)}) copy-start(f32[512,2]{0,1:T(2,128)} %get-tuple-element.34) | copy-start | bytes 12292
  21.6 30.3 %copy-start.16 = (pred[8]{0:T(512)(128)(4,1)S(1)}, pred[8]{0:T(512)(128)(4,1)}, u32[]{:S(2)}) copy-start(pred[8]{0:T(512)(128)(4,1)} %iota_compare_fusion.8) | copy-start | bytes 28
  53.6 3.1 %copy-start.5 = (bf16[512,256]{1,0:T(8,128)(2,1)S(1)}, bf16[512,256]{1,0:T(8,128)(2,1)}, u32[]{:S(2)}) copy-start(bf16[512,256]{1,0:T(8,128)(2,1)} %param.25) | copy-start | bytes 786436
  53.6 3.1 %copy-start.18 = (f32[256]{0:T(256)S(1)}, f32[256]{0:T(256)}, u32[]{:S(2)}) copy-start(f32[256]{0:T(256)} %param.32) | copy-start | bytes 3076
  53.6 7.4 %copy-start.14 = (f32[4]{0:T(128)S(1)}, f32[4]{0:T(128)}, u32[]{:S(2)}) copy-start(f32[4]{0:T(128)} %param.31) | copy-start | bytes 52
  53.6 7.8 %copy-start.17 = (pred[8]{0:T(512)(128)(4,1)S(1)}, pred[8]{0:T(512)(128)(4,1)}, u32[]{:S(2)}) copy-start(pred[8]{0:T(512)(128)(4,1)} %iota_compare_fusion.8) | copy-start | bytes 28
  55.8 7.2 %copy-start.3 = (bf16[512,4,32]{0,2,1:T(8,128)(2,1)S(1)}, bf16[512,4,32]{0,2,1:T(8,128)(2,1)}, u32[]{:S(2)}) copy-start(bf16[512,4,32]{0,2,1:T(8,128)(2,1)} %get-tuple-element.20) | copy-start | bytes 393220
  55.8 7.2 %copy-start.8 = (f32[512,4,32]{0,2,1:T(8,128)S(1)}, f32[512,4,32]{0,2,1:T(8,128)}, u32[]{:S(2)}) copy-start(f32[512,4,32]{0,2,1:T(8,128)} %copy-done.7) | copy-start | bytes 786436
  56.3 6.6 %copy-start.10 = (f32[512,4,32]{0,2,1:T(8,128)S(1)}, f32[512,4,32]{0,2,1:T(8,128)}, u32[]{:S(2)}) copy-start(f32[512,4,32]{0,2,1:T(8,128)} %copy-done.9) | copy-start | bytes 786436
  56.4 6.6 %copy-start.12 = (pred[512,512]{1,0:T(8,128)(4,1)S(1)}, pred[512,512]{1,0:T(8,128)(4,1)}, u32[]{:S(2)}) copy-start(pred[512,512]{1,0:T(8,128)(4,1)} %iota_compare_fusion) | copy-start | bytes 786436
  57.6 12.5 %all-to-all-start = ((bf16[4,128,256]{2,1,0:T(8,128)(2,1)}), bf16[4,128,256]{2,1,0:T(8,128)(2,1)S(1)}, u32[]{:S(2)}, u32[]{:S(2)}) async-start(bf16[4,128,256]{2,1,0:T(8,128)(2,1)} %bitcast.22), calls=%async_computation | async-start | bytes 524288 | tf_op jit(solution)/shard_map/all_to_all | solution.py:585
  66.0 3.1 %copy-start.6 = (bf16[512,256]{1,0:T(8,128)(2,1)S(1)}, bf16[512,256]{1,0:T(8,128)(2,1)}, u32[]{:S(2)}) copy-start(bf16[512,256]{1,0:T(8,128)(2,1)} %param.29) | copy-start | bytes 786436
  66.0 3.1 %copy-start.19 = (f32[256]{0:T(256)S(1)}, f32[256]{0:T(256)}, u32[]{:S(2)}) copy-start(f32[256]{0:T(256)} %param.33) | copy-start | bytes 3076
  69.2 13.7 %copy-start.2 = (bf16[128,2048]{1,0:T(8,128)(2,1)S(1)}, bf16[128,2048]{1,0:T(8,128)(2,1)}, u32[]{:S(2)}) copy-start(bf16[128,2048]{1,0:T(8,128)(2,1)} %param.37) | copy-start | bytes 1572868
  70.0 9.5 %all-to-all-start.1 = ((bf16[4,128,256]{2,1,0:T(8,128)(2,1)}), bf16[4,128,256]{2,1,0:T(8,128)(2,1)S(1)}, u32[]{:S(2)}, u32[]{:S(2)}) async-start(bf16[4,128,256]{2,1,0:T(8,128)(2,1)} %bitcast.29), calls=%async_computation.1 | async-start | bytes 524288 | tf_op jit(solution)/shard_map/all_to_all | solution.py:586
  79.7 3.5 %copy-start.1 = (bf16[1024,2048]{1,0:T(8,128)(2,1)S(1)}, bf16[1024,2048]{1,0:T(8,128)(2,1)}, u32[]{:S(2)}) copy-start(bf16[1024,2048]{1,0:T(8,128)(2,1)} %param.36) | copy-start | bytes 12582916
  82.8 1.2 copy-start.13

commit v2 on v1

--- a/solution.py
+++ b/solution.py
@@ -1,5 +1,6 @@
 import jax
 import jax.numpy as jnp
+import numpy as np
 from jax import lax
 from jax.experimental import pallas as pl
 from jax.experimental.pallas import tpu as pltpu
@@ -80,13 +81,51 @@
     return group, x, y, core, near, side, twin, far
 
 
-def experts_kernel(
-    rows_ref,
-    shares_ref,
+def layer_kernel(
+    inputs,
+    tables_ref,
+    turn_ref,
+    surge_ref,
+    wide_rate,
+    slim_rate,
+    wide_gain,
+    slim_gain,
+    wide_proj,
+    slim_proj,
+    skip_ref,
+    premix_ref,
+    ids_ref,
+    share_ref,
     valve_ref,
     expand_ref,
     contract_ref,
     out_ref,
+    staged,
+    tables,
+    proj,
+    skip,
+    queries,
+    keys,
+    faded,
+    level,
+    inner,
+    gates,
+    grown,
+    grown_out,
+    grown_in,
+    tile_out,
+    tiles,
+    plane_out,
+    plane_in,
+    carry_out,
+    carry_in,
+    mixed_out,
+    mixed,
+    updated,
+    normed,
+    holds,
+    rows,
+    returned,
     slots,
     valve,
     expand,
@@ -101,6 +140,16 @@
     load_sem,
     swap_send,
     swap_recv,
+    tile_send,
+    tile_recv,
+    grown_send,
+    grown_recv,
+    plane_send,
+    plane_recv,
+    carry_send,
+    carry_recv,
+    mixed_send,
+    mixed_recv,
     far_send,
     far_recv,
     near_send,
@@ -110,11 +159,40 @@
     home_send,
     home_recv,
 ):
-    groups, cap, width = rows_ref.shape
+    f32 = jnp.float32
+    bf16 = jnp.bfloat16
+    groups, cap, width = rows.shape
     units = valve_ref.shape[1]
+    length = staged.shape[1]
+    part = skip.shape[0]
+    lanes = 128
+    blocks = length // part
+    count = tiles.shape[0]
+    sp = lax.axis_index("sp")
+    tp = lax.axis_index("tp")
     group, x, y, core, near, side, twin, far = places_of(groups)
+    partner = sp + 1 - 2 * x
+    across = tp + 2 - 4 * y
+    twin_tp = tp + 1 - 2 * core
+    across_twin = twin_tp + 2 - 4 * y
+
+    loads = {}
+
+    def load(name, src, dst):
+        copy = pltpu.make_async_copy(src, dst, load_sem.at[len(loads)])
+        copy.start()
+        loads[name] = copy
+
+    for index in (1, 5):
+        load(index, inputs[index], staged.at[index])
+    load("tables", tables_ref, tables)
+    for index in (2, 6, 0, 4, 3, 7):
+        load(index, inputs[index], staged.at[index])
+    load("skip", skip_ref, skip)
+
     barrier = pltpu.get_barrier_semaphore()
-    friends = [near, side, twin] + far[1:]
+    friends = [{"sp": lax.rem(sp + step, count), "tp": tp} for step in range(1, count)]
+    friends += [{"sp": sp, "tp": other} for other in (across, twin_tp, across_twin)]
     for friend in friends:
         pl.semaphore_signal(barrier, inc=1, device_id=friend, device_id_type=MESH)
     pl.semaphore_wait(barrier, len(friends))
@@ -133,11 +211,389 @@
         sent.append(copy)
         return copy
 
+    def iota(shape, axis):
+        return lax.broadcasted_iota(jnp.int32, shape, axis)
+
+    lane = iota((part, lanes), 1)
+    row = iota((part, lanes), 0)
+    eye = lane == row
+    low_lane = iota((1, lanes), 1) < lanes // 2
+
+    surge = surge_ref[...]
+    wide_lane = iota((part, length), 1)
+    wide_row = iota((part, length), 0)
+    lines = []
+    for block in range(blocks):
+        column = jnp.sum(
+            jnp.where(wide_lane <= wide_row + block * part, surge, 0.0), 1, keepdims=True
+        )
+        level[pl.ds(block * part, part), :] = jnp.broadcast_to(column, (part, lanes))
+        lines.append(jnp.sum(jnp.where(eye, column, 0.0), 0, keepdims=True))
+    surge_line = jnp.concatenate(lines, 1)
+    surge_total = jnp.broadcast_to(jnp.sum(surge, 1, keepdims=True), (1, lanes))
+
+    rates = [
+        jnp.full((1, lanes), wide_rate[0], f32),
+        jnp.full((1, lanes), wide_rate[1], f32),
+        jnp.where(low_lane, slim_rate[0], slim_rate[1]),
+        jnp.where(low_lane, slim_rate[2], slim_rate[3]),
+    ]
+
+    def route(block):
+        begin = pl.multiple_of(block * part, part)
+        ids = ids_ref[pl.ds(begin, part), :]
+        weights = share_ref[pl.ds(begin, part), :]
+        first = ids[:, 0:1]
+        chosen = lax.shift_right_logical(first, 1)
+        named = chosen == lane
+        rank = jnp.dot(
+            jnp.where(row >= lane, 1.0, 0.0).astype(bf16),
+            jnp.where(named, 1.0, 0.0).astype(bf16),
+            preferred_element_type=f32,
+        )
+        order_in = jnp.sum(jnp.where(named, rank, 0.0), 1, keepdims=True).astype(jnp.int32) - 1
+        even = first - 2 * chosen == 0
+        shares = [
+            jnp.where(even, weights[:, 0:1], weights[:, 1:2]),
+            jnp.where(even, weights[:, 1:2], weights[:, 0:1]),
+        ]
+        return chosen, order_in, shares
+
+    chosen, order_in, _ = route(tp)
+    holds[...] = jnp.where(
+        chosen * cap + order_in == iota((part, groups * cap), 1), 1.0, 0.0
+    ).astype(bf16)
+    share_lines = [0.0, 0.0]
+    for block_y in range(2):
+        chosen, order_in, shares = route(2 * block_y + core)
+        here = chosen * (2 * cap) + block_y * cap + order_in == iota((part, 2 * groups * cap), 1)
+        for member in range(2):
+            share_lines[member] = share_lines[member] + jnp.sum(
+                jnp.where(here, shares[member], 0.0), 0, keepdims=True
+            )
+    top = iota((8, lanes), 0) == 0
+    for target in range(count):
+        line = share_lines[target % 2][:, (target // 2) * lanes : (target // 2 + 1) * lanes]
+        tile_out[target] = jnp.where(top, line, surge_total)
+    tile_copies = []
+    for step in range(1, count):
+        other = lax.rem(sp + step, count)
+        tile_copies.append(
+            send(
+                tile_out.at[other],
+                tiles.at[sp],
+                tile_send.at[step],
+                tile_recv.at[step],
+                {"sp": other, "tp": tp},
+            )
+        )
+    tiles[sp] = tile_out[sp]
+
+    def turner(size):
+        half = size // 2
+        low = lax.rem(lane, size) < half
+        match = row == jnp.where(low, lane + half, lane - half)
+        return jnp.where(match, jnp.where(low, -1.0, 1.0), 0.0).astype(bf16)
+
+    turns = [turner(BROAD_CHANNEL_DIM), turner(THIN_CHANNEL_DIM)]
+    scales = [BROAD_CHANNEL_DIM ** (-0.5), THIN_CHANNEL_DIM ** (-0.5)]
+    turn = turn_ref[sp]
+
+    def unit_of(index):
+        return index // 2, (index % 2) * lanes
+
+    loads["tables"].wait()
+    loads[1].wait()
+    loads[5].wait()
+    last = [rates[unit] * (length - 1) + surge_total for unit in range(4)]
+
+    def turn_keys(block, carry):
+        here = pl.ds(pl.multiple_of(block * part, part), part)
+        moment = (row + block * part).astype(f32)
+        summed = level[here, :]
+        for kind in range(2):
+            cosine_near = tables[2 * kind, here, :]
+            sine_near = tables[2 * kind + 1, here, :]
+            cosine_far = turn[2 * kind : 2 * kind + 1]
+            sine_far = turn[2 * kind + 1 : 2 * kind + 2]
+            cosine = cosine_near * cosine_far - sine_near * sine_far
+            sine = sine_near * cosine_far + cosine_near * sine_far
+            tables[2 * kind, here, :] = cosine
+            tables[2 * kind + 1, here, :] = sine
+            for index in range(2):
+                unit = 2 * kind + index
+                piece = staged[4 * kind + 1, here, index * lanes : (index + 1) * lanes]
+                turned = jnp.dot(piece, turns[kind], preferred_element_type=f32)
+                key = (
+                    (piece.astype(f32) * cosine + turned * sine) * scales[kind]
+                ).astype(bf16)
+                keys[unit, here, :] = key
+                tail = jnp.exp(last[unit] - (rates[unit] * moment + summed))
+                faded[unit, here, :] = (key.astype(f32) * tail).astype(bf16)
+        return carry
+
+    lax.fori_loop(0, blocks, turn_keys, 0)
+    loads[2].wait()
+    loads[6].wait()
+    for unit in range(4):
+        kind, begin = unit_of(unit)
+        change = lax.dot_general(
+            faded[unit],
+            staged[4 * kind + 2, :, begin : begin + lanes],
+            (((0,), (0,)), ((), ())),
+            preferred_element_type=f32,
+        )
+        half = unit % 2
+        if kind == 0:
+            grown[half, :lanes, :] = change
+            grown_out[half, :lanes, :] = change.astype(bf16)
+        else:
+            packed = jnp.where(low_lane, change[: lanes // 2], change[lanes // 2 :])
+            grown[half, lanes:, :] = packed
+            grown_out[half, lanes:, :] = packed.astype(bf16)
+    grown_copies = []
+    for index in range(2):
+        half = 1 - x if index == 0 else x
+        grown_copies.append(
+            send(
+                grown_out.at[half],
+                grown_in.at[half],
+                grown_send.at[index],
+                grown_recv.at[index],
+                {"sp": partner, "tp": tp},
+            )
+        )
+    load("wide_proj", wide_proj, proj.at[0])
+    load("slim_proj", slim_proj, proj.at[1])
+    swaps = []
+    for index, (src, dst) in enumerate(
+        ((valve_ref, valve), (expand_ref, expand), (contract_ref, contract))
+    ):
+        load(("expert", index), src, dst.at[core])
+        swaps.append(send(src, dst.at[core], swap_send.at[index], swap_recv.at[index], twin))
+
+    loads[0].wait()
+    loads[4].wait()
+
+    def turn_queries(block, carry):
+        here = pl.ds(pl.multiple_of(block * part, part), part)
+        for kind in range(2):
+            cosine = tables[2 * kind, here, :]
+            sine = tables[2 * kind + 1, here, :]
+            for index in range(2):
+                piece = staged[4 * kind, here, index * lanes : (index + 1) * lanes]
+                turned = jnp.dot(piece, turns[kind], preferred_element_type=f32)
+                queries[2 * kind + index, here, :] = (
+                    piece.astype(f32) * cosine + turned * sine
+                ).astype(bf16)
+        return carry
+
+    lax.fori_loop(0, blocks, turn_queries, 0)
+
+    def attend(unit):
+        kind, begin = unit_of(unit)
+        for block in range(blocks):
+            upto = (block + 1) * part
+            here = pl.ds(block * part, part)
+            query = queries[unit, here, :]
+            key = keys[unit, :upto, :]
+            value = staged[4 * kind + 2, :upto, begin : begin + lanes]
+            spots = iota((part, upto), 1)
+            times = iota((part, upto), 0) + block * part
+            causal = spots <= times
+            apart = (times - spots).astype(f32)
+            drop = level[here, 0:1] - surge_line[:, :upto]
+            results = []
+            for head in range(1 + kind):
+                if kind == 0:
+                    rate = wide_rate[unit]
+                    asked = query
+                else:
+                    rate = slim_rate[2 * (unit - 2) + head]
+                    mine = low_lane if head == 0 else jnp.logical_not(low_lane)
+                    asked = jnp.where(mine, query.astype(f32), 0.0).astype(bf16)
+                scores = lax.dot_general(
+                    asked, key, (((1,), (1,)), ((), ())), preferred_element_type=f32
+                )
+                gap = apart * rate + drop
+                decay = jnp.where(causal, jnp.exp(jnp.where(causal, gap, 0.0)), 0.0)
+                results.append(
+                    jnp.dot((scores * decay).astype(bf16), value, preferred_element_type=f32)
+                )
+            result = results[0] if kind == 0 else jnp.where(low_lane, results[0], results[1])
+            inner[here, unit * lanes : (unit + 1) * lanes] = result
+
+    attend(0)
+    attend(1)
+
+    for copy in tile_copies:
+        copy.wait_recv()
+
+    def block_level(place, unit):
+        return rates[unit] * length + tiles[place, 1:2, :]
+
+    grown_copies[0].wait_recv()
+    mine = grown[x]
+    other = grown_in[x].astype(f32)
+    first = jnp.where(x == 0, mine, other)
+    second = jnp.where(x == 0, other, mine)
+
+    def by_half(wide_values, slim_values):
+        return (
+            jnp.where(x == 0, wide_values[0], wide_values[1]),
+            jnp.where(x == 0, slim_values[0], slim_values[1]),
+        )
+
+    def weigh(value, pair):
+        return jnp.concatenate([value[:lanes] * pair[0], value[lanes:] * pair[1]], 0)
+
+    odd = [jnp.exp(block_level(2 * group + 1, unit)) for unit in range(4)]
+    plane_out[...] = (weigh(first, by_half(odd[:2], odd[2:])) + second).astype(bf16)
+    plane_copies = []
+    for step in range(1, groups):
+        plane_copies.append(
+            send(
+                plane_out,
+                plane_in.at[step],
+                plane_send.at[step],
+                plane_recv.at[step],
+                far[step],
+            )
+        )
+
+    attend(2)
+    attend(3)
+    loads[3].wait()
+    loads[7].wait()
+
+    def open_gates(block, carry):
+        here = pl.ds(pl.multiple_of(block * part, part), part)
+        for kind, gain in enumerate((wide_gain, slim_gain)):
+            gate = staged[4 * kind + 3, here, :].astype(f32)
+            gates[here, 2 * kind * lanes : (2 * kind + 2) * lanes] = gain[...] * jax.nn.silu(gate)
+        return carry
+
+    lax.fori_loop(0, blocks, open_gates, 0)
+    loads["skip"].wait()
+    updated[...] = skip[...].astype(f32)
+
+    carry = jnp.zeros(plane_out.shape, f32)
+    reach = [jnp.zeros((1, lanes), f32) for _ in range(4)]
+    for step in range(1, groups):
+        weight = [jnp.where(group >= step, jnp.exp(reach[unit]), 0.0) for unit in range(4)]
+        plane_copies[step - 1].wait_recv()
+        carry = carry + weigh(
+            plane_in[step].astype(f32), by_half(weight[:2], weight[2:])
+        )
+        place = lax.rem(group + groups - step, groups)
+        for unit in range(4):
+            reach[unit] = (
+                reach[unit] + block_level(2 * place, unit) + block_level(2 * place + 1, unit)
+            )
+    carry_out[...] = carry.astype(bf16)
+    carry_copy = send(
+        carry_out, carry_in, carry_send.at[0], carry_recv.at[0], {"sp": partner, "tp": tp}
+    )
+    grown_copies[1].wait_recv()
+    beside = [
+        jnp.where(x == 0, 1.0, jnp.exp(block_level(partner, unit))) for unit in range(4)
+    ]
+    earlier = jnp.where(x == 0, 0.0, 1.0)
+    carry_copy.wait_recv()
+    states = [None] * 4
+    for half in range(2):
+        held = jnp.where(x == half, carry, carry_in[...].astype(f32))
+        state = weigh(held, (beside[half], beside[2 + half])) + earlier * grown_in[half].astype(f32)
+        states[half] = state[:lanes].astype(bf16)
+        slim = state[lanes:]
+        states[2 + half] = jnp.concatenate(
+            [jnp.where(low_lane, slim, 0.0), jnp.where(low_lane, 0.0, slim)], 0
+        ).astype(bf16)
+
+    mixed_copies = []
+    for index, owner in enumerate((across, across_twin, twin_tp, tp)):
+        begin = pl.multiple_of(owner * part, part)
+        here = pl.ds(begin, part)
+        moment = (row + begin + 1).astype(f32)
+        summed = level[here, :]
+        for unit in range(4):
+            columns = slice(unit * lanes, (unit + 1) * lanes)
+            read = jnp.dot(queries[unit, here, :], states[unit], preferred_element_type=f32)
+            factor = jnp.exp(rates[unit] * moment + summed)
+            value = inner[here, columns] + factor * read
+            square = value * value
+            if unit < 2:
+                mean = jnp.sum(square, 1, keepdims=True) * (1.0 / BROAD_CHANNEL_DIM)
+            else:
+                mean = jnp.where(
+                    low_lane,
+                    jnp.sum(jnp.where(low_lane, square, 0.0), 1, keepdims=True),
+                    jnp.sum(jnp.where(low_lane, 0.0, square), 1, keepdims=True),
+                ) * (1.0 / THIN_CHANNEL_DIM)
+            gated = (value * lax.rsqrt(mean + epsilon) * gates[here, columns]).astype(bf16)
+            if index < 3:
+                mixed_out[index, :, columns] = gated
+            else:
+                mixed[tp, :, columns] = gated
+        if index < 3:
+            mixed_copies.append(
+                send(
+                    mixed_out.at[index],
+                    mixed.at[tp],
+                    mixed_send.at[index],
+                    mixed_recv.at[index],
+                    {"sp": sp, "tp": owner},
+                )
+            )
+
+    loads["wide_proj"].wait()
+    loads["slim_proj"].wait()
+    stride = 512
+    share_rows = 2 * lanes
+
+    def project(origin):
+        above = pl.ds(pl.multiple_of(origin * share_rows, share_rows), share_rows)
+        wide = mixed[origin, :, :share_rows]
+        slim = mixed[origin, :, share_rows:]
+
+        def one(index, carry):
+            column = pl.ds(pl.multiple_of(index * stride, stride), stride)
+            updated[:, column] += jnp.dot(
+                wide, proj[0, above, column], preferred_element_type=f32
+            ) + jnp.dot(slim, proj[1, above, column], preferred_element_type=f32)
+            return carry
+
+        lax.fori_loop(0, width // stride, one, 0)
+
+    project(tp)
+    mixed_copies[2].wait_recv()
+    project(twin_tp)
+    mixed_copies[0].wait_recv()
+    project(across)
+    mixed_copies[1].wait_recv()
+    project(across_twin)
+    square = jnp.zeros((part, lanes), f32)
+    for begin in range(0, width, lanes):
+        piece = updated[:, begin : begin + lanes]
+        square = square + piece * piece
+    scale = lax.rsqrt(jnp.sum(square, 1, keepdims=True) * (1.0 / width) + epsilon)
+
+    def place_rows(index, carry):
+        column = pl.ds(pl.multiple_of(index * stride, stride), stride)
+        piece = (updated[:, column] * scale * premix_ref[:, column]).astype(bf16)
+        spread_rows = lax.dot_general(
+            holds[...], piece, (((0,), (0,)), ((), ())), preferred_element_type=f32
+        )
+        rows[:, :, column] = spread_rows.reshape(groups, cap, stride).astype(bf16)
+        return carry
+
+    lax.fori_loop(0, width // stride, place_rows, 0)
+
     order = [0, 1, 3, 2]
     arriving = {}
     for step in order[1:]:
         arriving[step] = send(
-            rows_ref.at[lax.rem(group + step, groups)],
+            rows.at[lax.rem(group + step, groups)],
             slots.at[step, 0],
             far_send.at[step],
             far_recv.at[step],
@@ -148,7 +604,7 @@
     def spread(step):
         if step > 0:
             arriving[step].wait_recv()
-        src = rows_ref.at[group] if step == 0 else slots.at[step, 0]
+        src = rows.at[group] if step == 0 else slots.at[step, 0]
         own[step] = [
             send(src, slots.at[step, 1], near_send.at[step, 0], near_recv.at[step, 0], near),
             send(src, slots.at[step, 2], near_send.at[step, 1], near_recv.at[step, 1], side),
@@ -167,35 +623,22 @@
         )
 
     spread(0)
-    loads = []
-    swaps = []
-    for index, (src, dst) in enumerate(
-        ((valve_ref, valve), (expand_ref, expand), (contract_ref, contract))
-    ):
-        load = pltpu.make_async_copy(src, dst.at[core], load_sem.at[index])
-        load.start()
-        loads.append(load)
-        swaps.append(send(src, dst.at[core], swap_send.at[index], swap_recv.at[index], twin))
-    slots[0, 0] = rows_ref[group]
+    slots[0, 0] = rows[group]
     forward(0)
     spread(order[1])
+    near_x = 1 - x + core * (2 * x - 1)
+    near_y = y + core * (1 - 2 * y)
 
     def shares_for(step):
         origin = lax.rem(group + groups - step, groups)
-        near_x = 1 - x + core * (2 * x - 1)
-        near_y = y + core * (1 - 2 * y)
-        return jnp.concatenate(
-            [
-                shares_ref[origin, x, y],
-                shares_ref[origin, near_x, near_y],
-                shares_ref[origin, 1 - near_x + 0 * x, 1 - near_y],
-                shares_ref[origin, 1 - x, 1 - y],
-            ],
-            0,
-        )
+        found = []
+        for at_x, at_y in ((x, y), (near_x, near_y), (1 - near_x, 1 - near_y), (1 - x, 1 - y)):
+            line = tiles[2 * origin + at_x, 0:1, :]
+            pick = iota((cap, lanes), 1) == iota((cap, lanes), 0) + at_y * cap
+            found.append(jnp.sum(jnp.where(pick, line, 0.0), 1, keepdims=True))
+        return jnp.concatenate(found, 0)
 
     tile = 256
-    across = 512
 
     def widen(step):
         share = shares_for(step)
@@ -204,60 +647,52 @@
         def one(index, carry):
             half = index // (units // tile)
             begin = pl.multiple_of(lax.rem(index, units // tile) * tile, tile)
-            gate = jnp.dot(
-                batch, valve[half, :, pl.ds(begin, tile)], preferred_element_type=jnp.float32
-            )
-            up = jnp.dot(
-                batch, expand[half, :, pl.ds(begin, tile)], preferred_element_type=jnp.float32
-            )
+            gate = jnp.dot(batch, valve[half, :, pl.ds(begin, tile)], preferred_element_type=f32)
+            up = jnp.dot(batch, expand[half, :, pl.ds(begin, tile)], preferred_element_type=f32)
             place = pl.multiple_of(index * tile, tile)
-            hidden[:, pl.ds(place, tile)] = (jax.nn.silu(gate) * up * share).astype(hidden.dtype)
+            hidden[:, pl.ds(place, tile)] = (jax.nn.silu(gate) * up * share).astype(bf16)
             return carry
 
         lax.fori_loop(0, 2 * units // tile, one, 0)
+
+    folding = {}
+    joining = {}
+    homing = []
 
     def narrow(step):
         def one(index, carry):
-            begin = pl.multiple_of(index * across, across)
-            column = pl.ds(begin, across)
-            part = jnp.dot(
-                hidden[:, :units], contract[0, :, column], preferred_element_type=jnp.float32
-            ) + jnp.dot(
-                hidden[:, units:], contract[1, :, column], preferred_element_type=jnp.float32
-            )
-            kept[step, :, :, column] = part[: 2 * cap].reshape(2, cap, across)
-            leave[step, :, :, column] = part[2 * cap :].reshape(2, cap, across).astype(leave.dtype)
+            column = pl.ds(pl.multiple_of(index * stride, stride), stride)
+            made = jnp.dot(
+                hidden[:, :units], contract[0, :, column], preferred_element_type=f32
+            ) + jnp.dot(hidden[:, units:], contract[1, :, column], preferred_element_type=f32)
+            kept[step, :, :, column] = made[: 2 * cap].reshape(2, cap, stride)
+            leave[step, :, :, column] = made[2 * cap :].reshape(2, cap, stride).astype(bf16)
             return carry
 
-        lax.fori_loop(0, width // across, one, 0)
+        lax.fori_loop(0, width // stride, one, 0)
         folding[step] = send(
             leave.at[step], landed.at[step], fold_send.at[step, 0], fold_recv.at[step, 0], side
         )
 
-    folding = {}
-    joining = {}
-
     def join(step):
         folding[step].wait_recv()
-        joined[step] = (kept[step, 1] + landed[step, 1].astype(jnp.float32)).astype(joined.dtype)
+        joined[step] = (kept[step, 1] + landed[step, 1].astype(f32)).astype(bf16)
         joining[step] = send(
             joined.at[step], met.at[step], fold_send.at[step, 1], fold_recv.at[step, 1], near
         )
-        kept[step, 0] = kept[step, 0] + landed[step, 0].astype(jnp.float32)
-
-    homing = []
+        kept[step, 0] = kept[step, 0] + landed[step, 0].astype(f32)
 
     def finish_step(step):
         joining[step].wait_recv()
-        total = (kept[step, 0] + met[step].astype(jnp.float32)).astype(out_ref.dtype)
+        total = (kept[step, 0] + met[step].astype(f32)).astype(bf16)
         if step == 0:
-            out_ref[group] = total
+            returned[group] = total
         else:
             back[step] = total
             homing.append(
                 send(
                     back.at[step],
-                    out_ref.at[group],
+                    returned.at[group],
                     home_send.at[step],
                     home_recv.at[step],
                     far[groups - step],
@@ -268,9 +703,9 @@
         own[step][1].wait_recv()
         own[step][2].wait_recv()
         if place == 0:
-            for load, swap in zip(loads, swaps):
-                load.wait()
-                swap.wait_recv()
+            for index in range(3):
+                loads[("expert", index)].wait()
+                swaps[index].wait_recv()
         widen(step)
         if place + 1 < groups:
             forward(order[place + 1])
@@ -286,34 +721,116 @@
     finish_step(order[-1])
     for copy in homing:
         copy.wait_recv()
+
+    def close(index, carry):
+        column = pl.ds(pl.multiple_of(index * stride, stride), stride)
+        mixture = jnp.dot(
+            holds[...],
+            returned[:, :, column].reshape(groups * cap, stride),
+            preferred_element_type=f32,
+        )
+        out_ref[:, column] = (updated[:, column] + mixture).astype(bf16)
+        return carry
+
+    lax.fori_loop(0, width // stride, close, 0)
     for copy in sent:
         copy.wait_send()
 
 
-def experts_plane(rows, shares, valve, expand, contract):
-    groups, cap, width = rows.shape
+def rope_table(places):
+    found = []
+    for size in (BROAD_CHANNEL_DIM, THIN_CHANNEL_DIM):
+        half = size // 2
+        speed = rope_base ** (-np.arange(half, dtype=np.float64) * 2.0 / size)
+        angle = places.astype(np.float64)[:, None] * np.tile(speed, 128 // half)[None, :]
+        found += [np.cos(angle), np.sin(angle)]
+    return np.stack(found).astype(np.float32)
+
+
+def whole_layer(*arrays):
+    staged = arrays[:8]
+    (wide_rate, slim_rate, wide_gain, slim_gain, surge, wide_proj, slim_proj) = arrays[8:15]
+    (skip, premix, ids, shares, valve, expand, contract) = arrays[15:]
+    kind = skip.dtype
+    f32 = jnp.float32
+    length = surge.shape[0]
+    part, width = skip.shape
+    count = lax.axis_size("sp")
+    groups = GROUPS
+    cap = part * groups // count
+    valve, expand, contract = valve[0], expand[0], contract[0]
     units = valve.shape[1]
-    kind = rows.dtype
+    lanes = 128
+    near_table = jnp.asarray(rope_table(np.arange(length)))
+    far_table = jnp.asarray(rope_table(np.arange(count) * length).transpose(1, 0, 2))
     any_spec = pl.BlockSpec(memory_space=pl.ANY)
+    smem = pl.BlockSpec(memory_space=pltpu.SMEM)
     dma = pltpu.SemaphoreType.DMA
+    packed = lanes + lanes // 2
+
+    def kernel(*refs):
+        layer_kernel(refs[:8], *refs[8:])
+
     return pl.pallas_call(
-        experts_kernel,
-        out_shape=jax.ShapeDtypeStruct(rows.shape, kind),
-        in_specs=[VMEM_SPEC] * 2 + [any_spec] * 3,
+        kernel,
+        out_shape=jax.ShapeDtypeStruct(skip.shape, kind),
+        in_specs=[any_spec] * 9
+        + [VMEM_SPEC] * 2
+        + [smem] * 2
+        + [VMEM_SPEC] * 2
+        + [any_spec] * 3
+        + [VMEM_SPEC] * 3
+        + [any_spec] * 3,
         out_specs=VMEM_SPEC,
         scratch_shapes=[
+            pltpu.VMEM((8, length, 2 * lanes), kind),
+            pltpu.VMEM((4, length, lanes), f32),
+            pltpu.VMEM((2,) + wide_proj.shape, kind),
+            pltpu.VMEM((part, width), kind),
+            pltpu.VMEM((4, length, lanes), kind),
+            pltpu.VMEM((4, length, lanes), kind),
+            pltpu.VMEM((4, length, lanes), kind),
+            pltpu.VMEM((length, lanes), f32),
+            pltpu.VMEM((length, 4 * lanes), f32),
+            pltpu.VMEM((length, 4 * lanes), f32),
+            pltpu.VMEM((2, packed, lanes), f32),
+            pltpu.VMEM((2, packed, lanes), kind),
+            pltpu.VMEM((2, packed, lanes), kind),
+            pltpu.VMEM((count, 8, lanes), f32),
+            pltpu.VMEM((count, 8, lanes), f32),
+            pltpu.VMEM((packed, lanes), kind),
+            pltpu.VMEM((groups, packed, lanes), kind),
+            pltpu.VMEM((packed, lanes), kind),
+            pltpu.VMEM((packed, lanes), kind),
+            pltpu.VMEM((3, part, 4 * lanes), kind),
+            pltpu.VMEM((4, part, 4 * lanes), kind),
+            pltpu.VMEM((part, width), f32),
+            pltpu.VMEM((part, width), kind),
+            pltpu.VMEM((part, groups * cap), kind),
+            pltpu.VMEM((groups, cap, width), kind),
+            pltpu.VMEM((groups, cap, width), kind),
             pltpu.VMEM((groups, 4, cap, width), kind),
             pltpu.VMEM((2,) + valve.shape, kind),
             pltpu.VMEM((2,) + expand.shape, kind),
             pltpu.VMEM((2,) + contract.shape, kind),
             pltpu.VMEM((4 * cap, 2 * units), kind),
-            pltpu.VMEM((groups, 2, cap, width), jnp.float32),
+            pltpu.VMEM((groups, 2, cap, width), f32),
             pltpu.VMEM((groups, 2, cap, width), kind),
             pltpu.VMEM((groups, 2, cap, width), kind),
             pltpu.VMEM((groups, cap, width), kind),
             pltpu.VMEM((groups, cap, width), kind),
             pltpu.VMEM((groups, cap, width), kind),
+            dma((16,)),
             dma((3,)),
+            dma((3,)),
+            dma((count,)),
+            dma((count,)),
+            dma((2,)),
+            dma((2,)),
+            dma((groups,)),
+            dma((groups,)),
+            dma((1,)),
+            dma((1,)),
             dma((3,)),
             dma((3,)),
             dma((groups,)),
@@ -326,10 +843,28 @@
             dma((groups,)),
         ],
         compiler_params=pltpu.CompilerParams(
-            collective_id=3, has_side_effects=True, vmem_limit_bytes=56 * 1024 * 1024
+            collective_id=3, has_side_effects=True, vmem_limit_bytes=63 * 1024 * 1024
         ),
-        name="experts_plane",
-    )(rows, shares, valve, expand, contract)
+        name="whole_layer",
+    )(
+        *staged,
+        near_table,
+        far_table,
+        surge.reshape(1, -1),
+        wide_rate,
+        slim_rate,
+        wide_gain.reshape(1, -1),
+        slim_gain.reshape(1, -1),
+        wide_proj,
+        slim_proj,
+        skip,
+        premix.reshape(1, -1),
+        ids,
+        shares,
+        valve,
+        expand,
+        contract,
+    )
 
 
 def rotate(payload_tensor, positions):
@@ -466,20 +1001,14 @@
     return padded[source].reshape(experts, cap, rows_in.shape[1])
 
 
-def shares_by_slot(ids, shares, rows, cap):
-    core = lax.rem(lax.axis_index("tp"), 2)
-    ids = lax.dynamic_index_in_dim(ids.reshape(-1, 2, rows, 2), core, 1, False)
-    shares = lax.dynamic_index_in_dim(shares.reshape(-1, 2, rows, 2), core, 1, False)
-    group = ids[:, :, 0] // 2
-    named = group[:, :, None] == jnp.arange(GROUPS, dtype=jnp.int32)
-    rank = jnp.cumsum(named.astype(jnp.int32), 1) - 1
-    slot = group * cap + jnp.sum(jnp.where(named, rank, 0), 2)
-    holds = slot[:, None, :] == jnp.arange(GROUPS * cap, dtype=jnp.int32)[None, :, None]
-    found = []
-    for member in range(2):
-        share = jnp.sum(jnp.where(ids - 2 * group[:, :, None] == member, shares, 0.0), 2)
-        found.append(jnp.sum(jnp.where(holds, share[:, None, :], 0.0), 2))
-    return jnp.stack(found, 1).reshape(-1)
+def served(wide, slim, skip, valve):
+    return (
+        lax.axis_size("sp") * valve.shape[0] == 2 * GROUPS
+        and lax.axis_size("tp") == 4
+        and wide.shape[1] == slim.shape[1] == 2 * BROAD_CHANNEL_DIM
+        and skip.shape[0] == 128
+        and wide.shape[0] == 4 * skip.shape[0]
+    )
 
 
 def on_device(
@@ -508,13 +1037,34 @@
 ):
     length = broad_probe_tensor.shape[0]
     segment_begin = lax.axis_index("sp") * length
-    plane = lax.axis_size("sp") * specialist_valve_proj.shape[0] == 2 * GROUPS and (
-        lax.axis_size("tp") == 4
-    )
-    if not plane:
-        valve_all = lax.all_gather(specialist_valve_proj[0], "tp")
-        expand_all = lax.all_gather(specialist_expand_proj[0], "tp")
-        contract_all = lax.all_gather(specialist_contract_proj[0], "tp")
+    if served(broad_probe_tensor, slim_probe_tensor, skip_stream, specialist_valve_proj):
+        return whole_layer(
+            broad_probe_tensor,
+            broad_lookup_tensor,
+            broad_payload_tensor,
+            broad_emission_valve,
+            slim_probe_tensor,
+            slim_lookup_tensor,
+            slim_payload_tensor,
+            slim_emission_valve,
+            broad_forgetting_speed,
+            slim_forgetting_speed,
+            broad_channel_scaling,
+            slim_channel_scaling,
+            surge_forgetting,
+            broad_emission_proj,
+            slim_emission_proj,
+            skip_stream,
+            premix_scaling_coeffs,
+            routed_specialist_ids,
+            routed_specialist_shares,
+            specialist_valve_proj,
+            specialist_expand_proj,
+            specialist_contract_proj,
+        )
+    valve_all = lax.all_gather(specialist_valve_proj[0], "tp")
+    expand_all = lax.all_gather(specialist_expand_proj[0], "tp")
+    contract_all = lax.all_gather(specialist_contract_proj[0], "tp")
     wide_result = keeping_multiplier(
         broad_probe_tensor,
         broad_lookup_tensor,
@@ -544,15 +1094,6 @@
     )
     levels = jnp.concatenate([wide_result[3], narrow_result[3]])
     tile = levels
-    if plane:
-        group_of = own_ids[:, 0] // pair
-        named = group_of[:, None] == jnp.arange(GROUPS, dtype=jnp.int32)[None, :]
-        rank = jnp.cumsum(named.astype(jnp.int32), 0) - 1
-        own_slot = group_of * cap + jnp.sum(jnp.where(named, rank, 0), 1)
-        holds = own_slot[None, :] == jnp.arange(GROUPS * cap, dtype=jnp.int32)[:, None]
-        tile = jnp.concatenate(
-            [levels, shares_by_slot(routed_specialist_ids, routed_specialist_shares, rows, cap)]
-        )
     tile_size = -(-tile.shape[0] // 1024) * 1024
     tile = jnp.pad(tile, (0, tile_size - tile.shape[0])).reshape(-1, 128)
     packed = jnp.concatenate(
@@ -592,25 +1133,6 @@
     updated = skip_stream.astype(jnp.float32) + projected
     scale = lax.rsqrt(jnp.mean(updated * updated, -1, keepdims=True) + epsilon)
     normed = (updated * scale * premix_scaling_coeffs[None, :]).astype(jnp.bfloat16)
-    if plane:
-        spread = holds.astype(jnp.bfloat16)
-        filled = jnp.dot(spread, normed, preferred_element_type=jnp.float32).astype(jnp.bfloat16)
-        shares = tiles[:, both_heads : both_heads + 4 * GROUPS * cap]
-        shares = shares.reshape(GROUPS, 2, 2, 2, GROUPS, cap)
-        place = lax.axis_index("sp")
-        shares = lax.dynamic_index_in_dim(shares, place % 2, 3, False)
-        shares = lax.dynamic_index_in_dim(shares, place // 2, 3, False)
-        returned = experts_plane(
-            filled.reshape(GROUPS, cap, width),
-            shares[..., None],
-            specialist_valve_proj[0],
-            specialist_expand_proj[0],
-            specialist_contract_proj[0],
-        ).reshape(-1, width)
-        mixture = lax.dot_general(
-            spread, returned, (((0,), (0,)), ((), ())), preferred_element_type=jnp.float32
-        )
-        return (updated + mixture).astype(jnp.bfloat16)
     own_places = slot_positions(own_ids, experts, cap)
     slots = lax.all_to_all(
         fill_slots(normed, own_ids, experts, cap), "sp", split_axis=0, concat_axis=0, tiled=True

time: 189 us -> 126 us (0.67)
  other arithmetic: 22.9 us -> 0 us
  matrix products: 15.7 us -> 0 us
  local copies, waits for them, and re-layouts: 14.2 us -> 4.96 us
  starting transfers between devices: 6.99 us -> 0 us
  waiting for transfers between devices: 5.74 us -> 0 us
    dot_general x10 -> x0, matrix products: 15.7 us -> none  [the longest x2 5.19 us: segment_terms(): jnp.einsum('htm,mhe->the', weights, payload_tensor, preferred_element_typ...]
    all_to_all x2 -> x0, starting transfers between devices: 6.99 us -> none  [the longest x1 3.59 us: on_device(): lax.all_to_all(mixed_narrow, 'tp', split_axis=0, concat_axis=1, tiled=True)]
    all_to_all x2 -> x0, waiting for transfers between devices: 5.74 us -> none  [the longest x1 5.74 us: on_device(): lax.all_to_all(mixed_narrow, 'tp', split_axis=0, concat_axis=1, tiled=True)]
    add x8 -> x0, other arithmetic: 5.33 us -> none  [the longest x4 2.84 us: segment_terms(): forgetting_speed[None, :] * segment_tally[:, None]]
    another operation x8 -> x0, other arithmetic: 4.46 us -> none
    reshape x9 -> x0, local copies, waits for them, and re-layouts: 3.83 us -> none  [the longest x1 1.09 us: keeping_multiplier(): lookup_tensor.astype(jnp.float32).reshape(length, heads, channel_dimension)]
    reduce_sum x8 -> x0, other arithmetic: 3.19 us -> none  [the longest x2 2.41 us: carried(): return jnp.sum(weight[:, :, None, None] * states.astype(jnp.float32), 0)]
    cos x2 -> x0, other arithmetic: 2.78 us -> none  [rotate(): cosine = jnp.cos(angle)]
  transfers between devices with their start and end apart: 2 -> 0, of which waited for: 1 -> 0; matrix products, arithmetic and copies ran while one was open for 5% -> 0% of each run, Pallas kernels for 0% -> 0%
where the time goes in v2:
time: 126 us
  Pallas kernels  121 us (96%)
  local copies, waits for them, and re-layouts  4.96 us (4%)
    pallas_call x1, Pallas kernels, whole_layer(): pl.pallas_call(kernel, out_shape=jax.ShapeDtypeStruct(skip.shape, kind),...  121 us
    unnamed x3, local copies, waits for them, and re-layouts  4.96 us

profile of v2, /device:TPU:0, one launch (start us, length us, event | category | flops | bytes accessed | tf_op | source)
XLA Modules:
  0.0 125.5 jit_solution(6801889883480740814)
XLA Ops:
  0.0 1.5 %copy.25.refs_19_ = s32[512,2]{1,0:T(8,128)} copy(s32[512,2]{0,1:T(2,128)} %param.41) | data formatting | bytes 8192 | tf_op args[17]
  1.5 1.5 %copy.26.refs_20_ = f32[512,2]{1,0:T(8,128)} copy(f32[512,2]{0,1:T(2,128)} %param.42) | data formatting | bytes 8192 | tf_op args[18]
  3.1 120.6 %whole_layer.1 = bf16[128,2048]{1,0:T(8,128)(2,1)} custom-call(bf16[512,256]{1,0:T(8,128)(2,1)} %refs_0_.1, bf16[512,256]{1,0:T(8,128)(2,1)} %refs_1_.1, bf16[512,256]{1,0:T(8,128)(2,1)} %refs_2_.1, bf16[512,256]{1,0:T(8,128)(2,1)} %refs_3_.1, bf16[512,256]{1,0:T(8,128)(2,1)} %refs_4_.1, bf16[512,256]{1,0:T(8,128)(2,1)} %refs_5_.1, ...), custom_call_target="tpu_custom_call" | custom-call | tf_op jit(solution)/shard_map/whole_layer/pallas_call | solution.py:774
  123.7 1.9 %copy.28 = bf16[128,2048]{1,0:T(8,128)(2,1)} copy(bf16[128,2048]{1,0:T(8,128)(2,1)} %whole_layer.1) | data formatting | bytes 1048576

commit v3 on v2

--- a/solution.py
+++ b/solution.py
@@ -241,9 +241,13 @@
 
     def route(block):
         begin = pl.multiple_of(block * part, part)
-        ids = ids_ref[pl.ds(begin, part), :]
-        weights = share_ref[pl.ds(begin, part), :]
-        first = ids[:, 0:1]
+        ids = ids_ref[0:1, pl.ds(begin, part)]
+        weights = share_ref[:, pl.ds(begin, part)]
+        first = jnp.sum(jnp.where(eye, ids, 0), 1, keepdims=True)
+        weights = [
+            jnp.sum(jnp.where(eye, weights[choice : choice + 1], 0.0), 1, keepdims=True)
+            for choice in range(2)
+        ]
         chosen = lax.shift_right_logical(first, 1)
         named = chosen == lane
         rank = jnp.dot(
@@ -254,8 +258,8 @@
         order_in = jnp.sum(jnp.where(named, rank, 0.0), 1, keepdims=True).astype(jnp.int32) - 1
         even = first - 2 * chosen == 0
         shares = [
-            jnp.where(even, weights[:, 0:1], weights[:, 1:2]),
-            jnp.where(even, weights[:, 1:2], weights[:, 0:1]),
+            jnp.where(even, weights[0], weights[1]),
+            jnp.where(even, weights[1], weights[0]),
         ]
         return chosen, order_in, shares
 
@@ -589,42 +593,56 @@
 
     lax.fori_loop(0, width // stride, place_rows, 0)
 
-    order = [0, 1, 3, 2]
+    order = [1, 3, 2, 0]
+    piece_rows = cap // 2
+
+    def piece(portion):
+        return pl.ds(portion * piece_rows, piece_rows)
+
     arriving = {}
-    for step in order[1:]:
-        arriving[step] = send(
-            rows.at[lax.rem(group + step, groups)],
-            slots.at[step, 0],
-            far_send.at[step],
-            far_recv.at[step],
-            far[step],
-        )
+    for step in order[:3]:
+        for portion in range(2):
+            arriving[step, portion] = send(
+                rows.at[lax.rem(group + step, groups), piece(portion)],
+                slots.at[step, 0, piece(portion)],
+                far_send.at[step, portion],
+                far_recv.at[step, portion],
+                far[step],
+            )
     own = {}
 
     def spread(step):
-        if step > 0:
-            arriving[step].wait_recv()
-        src = rows.at[group] if step == 0 else slots.at[step, 0]
-        own[step] = [
-            send(src, slots.at[step, 1], near_send.at[step, 0], near_recv.at[step, 0], near),
-            send(src, slots.at[step, 2], near_send.at[step, 1], near_recv.at[step, 1], side),
-        ]
+        for portion in range(2):
+            here = piece(portion)
+            if step > 0:
+                arriving[step, portion].wait_recv()
+            src = rows.at[group, here] if step == 0 else slots.at[step, 0, here]
+            for place, device in ((1, near), (2, side)):
+                own[step, place, portion] = send(
+                    src,
+                    slots.at[step, place, here],
+                    near_send.at[step, 2 * place - 2 + portion],
+                    near_recv.at[step, 2 * place - 2 + portion],
+                    device,
+                )
 
     def forward(step):
-        own[step][0].wait_recv()
-        own[step].append(
-            send(
-                slots.at[step, 1],
-                slots.at[step, 3],
-                near_send.at[step, 2],
-                near_recv.at[step, 2],
+        for portion in range(2):
+            here = piece(portion)
+            own[step, 1, portion].wait_recv()
+            own[step, 3, portion] = send(
+                slots.at[step, 1, here],
+                slots.at[step, 3, here],
+                near_send.at[step, 4 + portion],
+                near_recv.at[step, 4 + portion],
                 side,
             )
-        )
 
     spread(0)
     slots[0, 0] = rows[group]
     forward(0)
+    spread(order[0])
+    forward(order[0])
     spread(order[1])
     near_x = 1 - x + core * (2 * x - 1)
     near_y = y + core * (1 - 2 * y)
@@ -640,7 +658,7 @@
 
     tile = 256
 
-    def widen(step):
+    def widen(step, portion):
         share = shares_for(step)
         batch = slots[step].reshape(4 * cap, width)
 
@@ -653,72 +671,113 @@
             hidden[:, pl.ds(place, tile)] = (jax.nn.silu(gate) * up * share).astype(bf16)
             return carry
 
-        lax.fori_loop(0, 2 * units // tile, one, 0)
+        count_tiles = 2 * units // tile // 2
+        lax.fori_loop(portion * count_tiles, (portion + 1) * count_tiles, one, 0)
 
     folding = {}
     joining = {}
     homing = []
+    span = width // 2
+
+    def columns_of(portion):
+        return pl.ds(portion * span, span)
 
     def narrow(step):
-        def one(index, carry):
-            column = pl.ds(pl.multiple_of(index * stride, stride), stride)
-            made = jnp.dot(
-                hidden[:, :units], contract[0, :, column], preferred_element_type=f32
-            ) + jnp.dot(hidden[:, units:], contract[1, :, column], preferred_element_type=f32)
-            kept[step, :, :, column] = made[: 2 * cap].reshape(2, cap, stride)
-            leave[step, :, :, column] = made[2 * cap :].reshape(2, cap, stride).astype(bf16)
-            return carry
-
-        lax.fori_loop(0, width // stride, one, 0)
-        folding[step] = send(
-            leave.at[step], landed.at[step], fold_send.at[step, 0], fold_recv.at[step, 0], side
-        )
+        for portion in range(2):
+
+            def one(index, carry):
+                column = pl.ds(pl.multiple_of(index * stride, stride), stride)
+                made = jnp.dot(
+                    hidden[:, :units], contract[0, :, column], preferred_element_type=f32
+                ) + jnp.dot(hidden[:, units:], contract[1, :, column], preferred_element_type=f32)
+                kept[step, :, :, column] = made[: 2 * cap].reshape(2, cap, stride)
+                leave[step, :, :, column] = made[2 * cap :].reshape(2, cap, stride).astype(bf16)
+                return carry
+
+            count_tiles = span // stride
+            lax.fori_loop(portion * count_tiles, (portion + 1) * count_tiles, one, 0)
+            column = columns_of(portion)
+            folding[step, portion] = send(
+                leave.at[step, :, :, column],
+                landed.at[step, :, :, column],
+                fold_send.at[step, portion],
+                fold_recv.at[step, portion],
+                side,
+            )
 
     def join(step):
-        folding[step].wait_recv()
-        joined[step] = (kept[step, 1] + landed[step, 1].astype(f32)).astype(bf16)
-        joining[step] = send(
-            joined.at[step], met.at[step], fold_send.at[step, 1], fold_recv.at[step, 1], near
-        )
-        kept[step, 0] = kept[step, 0] + landed[step, 0].astype(f32)
+        for portion in range(2):
+            column = columns_of(portion)
+            folding[step, portion].wait_recv()
+            joined[step, :, column] = (
+                kept[step, 1, :, column] + landed[step, 1, :, column].astype(f32)
+            ).astype(bf16)
+            joining[step, portion] = send(
+                joined.at[step, :, column],
+                met.at[step, :, column],
+                fold_send.at[step, 2 + portion],
+                fold_recv.at[step, 2 + portion],
+                near,
+            )
 
     def finish_step(step):
-        joining[step].wait_recv()
-        total = (kept[step, 0] + met[step].astype(f32)).astype(bf16)
-        if step == 0:
-            returned[group] = total
-        else:
-            back[step] = total
-            homing.append(
-                send(
-                    back.at[step],
-                    returned.at[group],
-                    home_send.at[step],
-                    home_recv.at[step],
-                    far[groups - step],
+        for portion in range(2):
+            column = columns_of(portion)
+            joining[step, portion].wait_recv()
+            total = (
+                kept[step, 0, :, column]
+                + landed[step, 0, :, column].astype(f32)
+                + met[step, :, column].astype(f32)
+            ).astype(bf16)
+            if step == 0:
+                returned[group, :, column] = total
+            else:
+                back[step, :, column] = total
+                homing.append(
+                    send(
+                        back.at[step, :, column],
+                        returned.at[group, :, column],
+                        home_send.at[step, portion],
+                        home_recv.at[step, portion],
+                        far[groups - step],
+                    )
                 )
-            )
-
-    for place, step in enumerate(order):
-        own[step][1].wait_recv()
-        own[step][2].wait_recv()
-        if place == 0:
-            for index in range(3):
-                loads[("expert", index)].wait()
-                swaps[index].wait_recv()
-        widen(step)
-        if place + 1 < groups:
-            forward(order[place + 1])
-        if place + 2 < groups:
-            spread(order[place + 2])
-        narrow(step)
-        if place >= 1:
-            join(order[place - 1])
-        if place >= 2:
-            finish_step(order[place - 2])
-    join(order[-1])
-    finish_step(order[-2])
-    finish_step(order[-1])
+
+    def gathered(step):
+        for portion in range(2):
+            own[step, 2, portion].wait_recv()
+            own[step, 3, portion].wait_recv()
+
+    for index in range(3):
+        loads[("expert", index)].wait()
+        swaps[index].wait_recv()
+    gathered(order[0])
+    widen(order[0], 0)
+    spread(order[2])
+    widen(order[0], 1)
+    forward(order[1])
+    narrow(order[0])
+    gathered(order[1])
+    widen(order[1], 0)
+    forward(order[2])
+    widen(order[1], 1)
+    narrow(order[1])
+    join(order[0])
+    gathered(order[2])
+    widen(order[2], 0)
+    finish_step(order[0])
+    widen(order[2], 1)
+    narrow(order[2])
+    join(order[1])
+    gathered(order[3])
+    widen(order[3], 0)
+    finish_step(order[1])
+    widen(order[3], 1)
+    narrow(order[3])
+    join(order[2])
+    finish_step(order[2])
+    join(order[3])
+    finish_step(order[3])
     for copy in homing:
         copy.wait_recv()
 
@@ -833,14 +892,14 @@
             dma((1,)),
             dma((3,)),
             dma((3,)),
-            dma((groups,)),
-            dma((groups,)),
-            dma((groups, 3)),
-            dma((groups, 3)),
             dma((groups, 2)),
             dma((groups, 2)),
-            dma((groups,)),
-            dma((groups,)),
+            dma((groups, 6)),
+            dma((groups, 6)),
+            dma((groups, 4)),
+            dma((groups, 4)),
+            dma((groups, 2)),
+            dma((groups, 2)),
         ],
         compiler_params=pltpu.CompilerParams(
             collective_id=3, has_side_effects=True, vmem_limit_bytes=63 * 1024 * 1024
@@ -859,8 +918,8 @@
         slim_proj,
         skip,
         premix.reshape(1, -1),
-        ids,
-        shares,
+        ids.T,
+        shares.T,
         valve,
         expand,
         contract,

time: 126 us -> 110 us (0.87)
  Pallas kernels: 121 us -> 108 us
  local copies, waits for them, and re-layouts: 4.96 us -> 1.88 us
    pallas_call x1, Pallas kernels: 121 us -> 108 us  [whole_layer(): pl.pallas_call(kernel, out_shape=jax.ShapeDtypeStruct(skip.shape, kind),...]
    unnamed x3 -> x1, local copies, waits for them, and re-layouts: 4.96 us -> 1.88 us
where the time goes in v3:
time: 110 us
  Pallas kernels  108 us (98%)
  local copies, waits for them, and re-layouts  1.88 us (2%)
    pallas_call x1, Pallas kernels, whole_layer(): pl.pallas_call(kernel, out_shape=jax.ShapeDtypeStruct(skip.shape, kind),...  108 us

profile of v3, /device:TPU:0, one launch (start us, length us, event | category | flops | bytes accessed | tf_op | source)
XLA Modules:
  0.0 109.9 jit_solution(3411358648055599243)
XLA Ops:
  0.0 108.0 %whole_layer.1 = bf16[128,2048]{1,0:T(8,128)(2,1)} custom-call(bf16[512,256]{1,0:T(8,128)(2,1)} %refs_0_.1, bf16[512,256]{1,0:T(8,128)(2,1)} %refs_1_.1, bf16[512,256]{1,0:T(8,128)(2,1)} %refs_2_.1, bf16[512,256]{1,0:T(8,128)(2,1)} %refs_3_.1, bf16[512,256]{1,0:T(8,128)(2,1)} %refs_4_.1, bf16[512,256]{1,0:T(8,128)(2,1)} %refs_5_.1, ...), custom_call_target="tpu_custom_call" | custom-call | tf_op jit(solution)/shard_map/whole_layer/pallas_call | solution.py:833
  108.0 1.9 %copy.26 = bf16[128,2048]{1,0:T(8,128)(2,1)} copy(bf16[128,2048]{1,0:T(8,128)(2,1)} %whole_layer.1) | data formatting | bytes 1048576

commit v4 on v3

--- a/solution.py
+++ b/solution.py
@@ -176,6 +176,12 @@
     twin_tp = tp + 1 - 2 * core
     across_twin = twin_tp + 2 - 4 * y
 
+    barrier = pltpu.get_barrier_semaphore()
+    friends = [{"sp": lax.rem(sp + step, count), "tp": tp} for step in range(1, count)]
+    friends += [{"sp": sp, "tp": other} for other in (across, twin_tp, across_twin)]
+    for friend in friends:
+        pl.semaphore_signal(barrier, inc=1, device_id=friend, device_id_type=MESH)
+
     loads = {}
 
     def load(name, src, dst):
@@ -190,12 +196,6 @@
         load(index, inputs[index], staged.at[index])
     load("skip", skip_ref, skip)
 
-    barrier = pltpu.get_barrier_semaphore()
-    friends = [{"sp": lax.rem(sp + step, count), "tp": tp} for step in range(1, count)]
-    friends += [{"sp": sp, "tp": other} for other in (across, twin_tp, across_twin)]
-    for friend in friends:
-        pl.semaphore_signal(barrier, inc=1, device_id=friend, device_id_type=MESH)
-    pl.semaphore_wait(barrier, len(friends))
     sent = []
 
     def send(src, dst, send_sem, recv_sem, device):
@@ -279,20 +279,6 @@
     for target in range(count):
         line = share_lines[target % 2][:, (target // 2) * lanes : (target // 2 + 1) * lanes]
         tile_out[target] = jnp.where(top, line, surge_total)
-    tile_copies = []
-    for step in range(1, count):
-        other = lax.rem(sp + step, count)
-        tile_copies.append(
-            send(
-                tile_out.at[other],
-                tiles.at[sp],
-                tile_send.at[step],
-                tile_recv.at[step],
-                {"sp": other, "tp": tp},
-            )
-        )
-    tiles[sp] = tile_out[sp]
-
     def turner(size):
         half = size // 2
         low = lax.rem(lane, size) < half
@@ -355,6 +341,20 @@
             packed = jnp.where(low_lane, change[: lanes // 2], change[lanes // 2 :])
             grown[half, lanes:, :] = packed
             grown_out[half, lanes:, :] = packed.astype(bf16)
+    pl.semaphore_wait(barrier, len(friends))
+    tile_copies = []
+    for step in range(1, count):
+        other = lax.rem(sp + step, count)
+        tile_copies.append(
+            send(
+                tile_out.at[other],
+                tiles.at[sp],
+                tile_send.at[step],
+                tile_recv.at[step],
+                {"sp": other, "tp": tp},
+            )
+        )
+    tiles[sp] = tile_out[sp]
     grown_copies = []
     for index in range(2):
         half = 1 - x if index == 0 else x
@@ -428,7 +428,6 @@
             inner[here, unit * lanes : (unit + 1) * lanes] = result
 
     attend(0)
-    attend(1)
 
     for copy in tile_copies:
         copy.wait_recv()
@@ -465,6 +464,7 @@
             )
         )
 
+    attend(1)
     attend(2)
     attend(3)
     loads[3].wait()
@@ -593,62 +593,76 @@
 
     lax.fori_loop(0, width // stride, place_rows, 0)
 
-    order = [1, 3, 2, 0]
+    order = [1, 2, 3, 0]
+    pairs = [lax.rem(group + groups - step, groups) for step in range(groups)]
+    seen_as = list(range(groups))
+    away = [{"sp": 2 * pairs[step] + x, "tp": tp} for step in range(groups)]
     piece_rows = cap // 2
 
     def piece(portion):
         return pl.ds(portion * piece_rows, piece_rows)
 
-    arriving = {}
     for step in order[:3]:
         for portion in range(2):
-            arriving[step, portion] = send(
+            send(
                 rows.at[lax.rem(group + step, groups), piece(portion)],
                 slots.at[step, 0, piece(portion)],
                 far_send.at[step, portion],
                 far_recv.at[step, portion],
                 far[step],
             )
+
+    def arrived(dst, recv_sem, step):
+        pltpu.make_async_remote_copy(
+            src_ref=dst,
+            dst_ref=dst,
+            send_sem=far_send.at[0, 0],
+            recv_sem=recv_sem,
+            device_id=away[step],
+            device_id_type=MESH,
+        ).wait_recv()
+
     own = {}
 
-    def spread(step):
-        for portion in range(2):
-            here = piece(portion)
-            if step > 0:
-                arriving[step, portion].wait_recv()
-            src = rows.at[group, here] if step == 0 else slots.at[step, 0, here]
-            for place, device in ((1, near), (2, side)):
-                own[step, place, portion] = send(
-                    src,
-                    slots.at[step, place, here],
-                    near_send.at[step, 2 * place - 2 + portion],
-                    near_recv.at[step, 2 * place - 2 + portion],
-                    device,
-                )
-
-    def forward(step):
-        for portion in range(2):
-            here = piece(portion)
-            own[step, 1, portion].wait_recv()
-            own[step, 3, portion] = send(
-                slots.at[step, 1, here],
-                slots.at[step, 3, here],
-                near_send.at[step, 4 + portion],
-                near_recv.at[step, 4 + portion],
-                side,
+    def spread(step, portion):
+        here = piece(portion)
+        if step > 0:
+            arrived(slots.at[step, 0, here], far_recv.at[step, portion], step)
+        src = rows.at[group, here] if step == 0 else slots.at[step, 0, here]
+        for place, device in ((1, near), (2, side)):
+            own[step, place, portion] = send(
+                src,
+                slots.at[step, place, here],
+                near_send.at[step, 2 * place - 2 + portion],
+                near_recv.at[step, 2 * place - 2 + portion],
+                device,
             )
 
-    spread(0)
+    def forward(step, portion):
+        here = piece(portion)
+        own[step, 1, portion].wait_recv()
+        own[step, 3, portion] = send(
+            slots.at[step, 1, here],
+            slots.at[step, 3, here],
+            near_send.at[step, 4 + portion],
+            near_recv.at[step, 4 + portion],
+            side,
+        )
+
+    spread(0, 0)
+    spread(0, 1)
     slots[0, 0] = rows[group]
-    forward(0)
-    spread(order[0])
-    forward(order[0])
-    spread(order[1])
+    forward(0, 0)
+    forward(0, 1)
+    spread(1, 0)
+    spread(1, 1)
+    forward(1, 0)
+    forward(1, 1)
     near_x = 1 - x + core * (2 * x - 1)
     near_y = y + core * (1 - 2 * y)
 
     def shares_for(step):
-        origin = lax.rem(group + groups - step, groups)
+        origin = pairs[step]
         found = []
         for at_x, at_y in ((x, y), (near_x, near_y), (1 - near_x, 1 - near_y), (1 - x, 1 - y)):
             line = tiles[2 * origin + at_x, 0:1, :]
@@ -668,7 +682,9 @@
             gate = jnp.dot(batch, valve[half, :, pl.ds(begin, tile)], preferred_element_type=f32)
             up = jnp.dot(batch, expand[half, :, pl.ds(begin, tile)], preferred_element_type=f32)
             place = pl.multiple_of(index * tile, tile)
-            hidden[:, pl.ds(place, tile)] = (jax.nn.silu(gate) * up * share).astype(bf16)
+            hidden[int(step == 0), :, pl.ds(place, tile)] = (
+                jax.nn.silu(gate) * up * share
+            ).astype(bf16)
             return carry
 
         count_tiles = 2 * units // tile // 2
@@ -676,27 +692,28 @@
 
     folding = {}
     joining = {}
-    homing = []
-    span = width // 2
-
-    def columns_of(portion):
+    chunks = {0: 2, 1: 2, 2: 2, 3: 2}
+
+    def columns_of(step, portion):
+        span = width // chunks[step]
         return pl.ds(portion * span, span)
 
-    def narrow(step):
-        for portion in range(2):
+    def narrow(step, portions):
+        for portion in portions:
 
             def one(index, carry):
                 column = pl.ds(pl.multiple_of(index * stride, stride), stride)
                 made = jnp.dot(
-                    hidden[:, :units], contract[0, :, column], preferred_element_type=f32
-                ) + jnp.dot(hidden[:, units:], contract[1, :, column], preferred_element_type=f32)
+                    hidden[int(step == 0), :, :units], contract[0, :, column], preferred_element_type=f32
+                ) + jnp.dot(
+                    hidden[int(step == 0), :, units:], contract[1, :, column], preferred_element_type=f32)
                 kept[step, :, :, column] = made[: 2 * cap].reshape(2, cap, stride)
                 leave[step, :, :, column] = made[2 * cap :].reshape(2, cap, stride).astype(bf16)
                 return carry
 
-            count_tiles = span // stride
-            lax.fori_loop(portion * count_tiles, (portion + 1) * count_tiles, one, 0)
-            column = columns_of(portion)
+            tiles_in = width // chunks[step] // stride
+            lax.fori_loop(portion * tiles_in, (portion + 1) * tiles_in, one, 0)
+            column = columns_of(step, portion)
             folding[step, portion] = send(
                 leave.at[step, :, :, column],
                 landed.at[step, :, :, column],
@@ -706,8 +723,8 @@
             )
 
     def join(step):
-        for portion in range(2):
-            column = columns_of(portion)
+        for portion in range(chunks[step]):
+            column = columns_of(step, portion)
             folding[step, portion].wait_recv()
             joined[step, :, column] = (
                 kept[step, 1, :, column] + landed[step, 1, :, column].astype(f32)
@@ -715,33 +732,34 @@
             joining[step, portion] = send(
                 joined.at[step, :, column],
                 met.at[step, :, column],
-                fold_send.at[step, 2 + portion],
-                fold_recv.at[step, 2 + portion],
+                fold_send.at[step, 4 + portion],
+                fold_recv.at[step, 4 + portion],
                 near,
             )
 
+    def finish_part(step, portion):
+        column = columns_of(step, portion)
+        joining[step, portion].wait_recv()
+        total = (
+            kept[step, 0, :, column]
+            + landed[step, 0, :, column].astype(f32)
+            + met[step, :, column].astype(f32)
+        ).astype(bf16)
+        if step == 0:
+            returned[group, :, column] = total
+        else:
+            back[step, :, column] = total
+            send(
+                back.at[step, :, column],
+                returned.at[group, :, column],
+                home_send.at[step, portion],
+                home_recv.at[seen_as[step], portion],
+                away[step],
+            )
+
     def finish_step(step):
-        for portion in range(2):
-            column = columns_of(portion)
-            joining[step, portion].wait_recv()
-            total = (
-                kept[step, 0, :, column]
-                + landed[step, 0, :, column].astype(f32)
-                + met[step, :, column].astype(f32)
-            ).astype(bf16)
-            if step == 0:
-                returned[group, :, column] = total
-            else:
-                back[step, :, column] = total
-                homing.append(
-                    send(
-                        back.at[step, :, column],
-                        returned.at[group, :, column],
-                        home_send.at[step, portion],
-                        home_recv.at[step, portion],
-                        far[groups - step],
-                    )
-                )
+        for portion in range(chunks[step]):
+            finish_part(step, portion)
 
     def gathered(step):
         for portion in range(2):
@@ -751,47 +769,53 @@
     for index in range(3):
         loads[("expert", index)].wait()
         swaps[index].wait_recv()
-    gathered(order[0])
-    widen(order[0], 0)
-    spread(order[2])
-    widen(order[0], 1)
-    forward(order[1])
-    narrow(order[0])
-    gathered(order[1])
-    widen(order[1], 0)
-    forward(order[2])
-    widen(order[1], 1)
-    narrow(order[1])
-    join(order[0])
-    gathered(order[2])
-    widen(order[2], 0)
-    finish_step(order[0])
-    widen(order[2], 1)
-    narrow(order[2])
-    join(order[1])
-    gathered(order[3])
-    widen(order[3], 0)
-    finish_step(order[1])
-    widen(order[3], 1)
-    narrow(order[3])
-    join(order[2])
-    finish_step(order[2])
-    join(order[3])
-    finish_step(order[3])
-    for copy in homing:
-        copy.wait_recv()
-
-    def close(index, carry):
-        column = pl.ds(pl.multiple_of(index * stride, stride), stride)
+    gathered(0)
+    widen(0, 0)
+    spread(3, 0)
+    spread(3, 1)
+    widen(0, 1)
+    spread(2, 0)
+    spread(2, 1)
+    gathered(1)
+    widen(1, 0)
+    forward(3, 0)
+    forward(3, 1)
+    widen(1, 1)
+    narrow(1, [0, 1])
+    gathered(3)
+    widen(3, 0)
+    forward(2, 0)
+    forward(2, 1)
+    widen(3, 1)
+    narrow(3, [0, 1])
+    join(1)
+    gathered(2)
+    widen(2, 0)
+    finish_step(1)
+    widen(2, 1)
+    narrow(2, [0, 1])
+    join(3)
+    narrow(0, [0, 1])
+    finish_step(3)
+    join(2)
+    finish_step(2)
+    join(0)
+    for step in range(1, groups):
+        for portion in range(chunks[step]):
+            arrived(
+                returned.at[lax.rem(group + step, groups), :, columns_of(step, portion)],
+                home_recv.at[step, portion],
+                step,
+            )
+    for portion in range(2):
+        finish_part(0, portion)
+        column = pl.ds(portion * (width // 2), width // 2)
         mixture = jnp.dot(
             holds[...],
-            returned[:, :, column].reshape(groups * cap, stride),
+            returned[:, :, column].reshape(groups * cap, -1),
             preferred_element_type=f32,
         )
         out_ref[:, column] = (updated[:, column] + mixture).astype(bf16)
-        return carry
-
-    lax.fori_loop(0, width // stride, close, 0)
     for copy in sent:
         copy.wait_send()
 
@@ -872,7 +896,7 @@
             pltpu.VMEM((2,) + valve.shape, kind),
             pltpu.VMEM((2,) + expand.shape, kind),
             pltpu.VMEM((2,) + contract.shape, kind),
-            pltpu.VMEM((4 * cap, 2 * units), kind),
+            pltpu.VMEM((2, 4 * cap, 2 * units), kind),
             pltpu.VMEM((groups, 2, cap, width), f32),
             pltpu.VMEM((groups, 2, cap, width), kind),
             pltpu.VMEM((groups, 2, cap, width), kind),
@@ -896,10 +920,10 @@
             dma((groups, 2)),
             dma((groups, 6)),
             dma((groups, 6)),
+            dma((groups, 8)),
+            dma((groups, 8)),
             dma((groups, 4)),
             dma((groups, 4)),
-            dma((groups, 2)),
-            dma((groups, 2)),
         ],
         compiler_params=pltpu.CompilerParams(
             collective_id=3, has_side_effects=True, vmem_limit_bytes=63 * 1024 * 1024

time: 110 us -> 108 us (0.982)
  Pallas kernels: 108 us -> 106 us
    pallas_call x1, Pallas kernels: 108 us -> 106 us  [whole_layer(): pl.pallas_call(kernel, out_shape=jax.ShapeDtypeStruct(skip.shape, kind),...]
where the time goes in v4:
time: 108 us
  Pallas kernels  106 us (98%)
  local copies, waits for them, and re-layouts  1.88 us (2%)
    pallas_call x1, Pallas kernels, whole_layer(): pl.pallas_call(kernel, out_shape=jax.ShapeDtypeStruct(skip.shape, kind),...  106 us

profile of v4, /device:TPU:0, one launch (start us, length us, event | category | flops | bytes accessed | tf_op | source)
XLA Modules:
  0.0 107.5 jit_solution(17211472866310654253)
XLA Ops:
  0.0 105.6 %whole_layer.1 = bf16[128,2048]{1,0:T(8,128)(2,1)} custom-call(bf16[512,256]{1,0:T(8,128)(2,1)} %refs_0_.1, bf16[512,256]{1,0:T(8,128)(2,1)} %refs_1_.1, bf16[512,256]{1,0:T(8,128)(2,1)} %refs_2_.1, bf16[512,256]{1,0:T(8,128)(2,1)} %refs_3_.1, bf16[512,256]{1,0:T(8,128)(2,1)} %refs_4_.1, bf16[512,256]{1,0:T(8,128)(2,1)} %refs_5_.1, ...), custom_call_target="tpu_custom_call" | custom-call | tf_op jit(solution)/shard_map/whole_layer/pallas_call | solution.py:857
  105.7 1.9 %copy.26 = bf16[128,2048]{1,0:T(8,128)(2,1)} copy(bf16[128,2048]{1,0:T(8,128)(2,1)} %whole_layer.1) | data formatting | bytes 1048576
